TPU v7x, 32 devices: a whole 2x2x4 slice. The times are simulated.
32 devices in a mesh: sp: 8 (over z, x), tp: 4 (over y, core).
Axes of the slice: x: 2, y: 2, z: 4, core: 2. Of those that a mesh axis runs over, the one named last changes fastest.
Arguments:
- tokens: bfloat16 [4096, 2048], P('sp', 'tp'), may hold values from -72 to 72
- w_query: bfloat16 [2048, 1024], P('sp', 'tp'), may hold values from -0.125 to 0.125
- w_key: bfloat16 [2048, 256], P('sp', 'tp'), may hold values from -0.125 to 0.125
- w_value: bfloat16 [2048, 256], P('sp', 'tp'), may hold values from -0.125 to 0.125
- w_pool_in: bfloat16 [2048, 1024], P('sp', 'tp'), may hold values from -0.125 to 0.125
- sink: float32 [16], P('tp'), may hold values from 3 to 7
- w_pool: bfloat16 [4, 256, 256], P('tp'), may hold values from -0.375 to 0.375
- pool_scale: float32 [1024], P('tp'), may hold values from 0.1 to 1.9
- w_out_attn: bfloat16 [1024, 2048], P('tp', 'sp'), may hold values from -0.5 to 0.5
- w_out_pool: bfloat16 [1024, 2048], P('tp', 'sp'), may hold values from -0.125 to 0.125
- out_gain: float32 [2048], P('tp'), may hold values from 0.1 to 1.9
Outputs:
- mixed: bfloat16 [4096, 2048], P('sp', 'tp')
All inputs are finite; a program needn't handle non-finite values.
Results may differ from a plain program's by a relative error of at most 0.012.
The roundings to bfloat16 on the way count: a program that leaves them out, or rounds other values in their place, can miss the bound.
Values may be sent and summed in bfloat16 or wider, within the bound.
A program may use at most 64 MiB of HBM per device.

v0:
```python
import functools

import jax
import jax.numpy as jnp
from jax import lax
from jax.experimental import pallas as pl
from jax.experimental.pallas import tpu as pltpu
from jax.sharding import PartitionSpec as P

HEAD_DIM = 64
POOL_GROUPS = 4
WINDOW = 128


epsilon = 1e-05
masked_score = -1e30


def padded(cells, sides, width):
    for axis, dim in sides:
        count = lax.axis_size(axis)
        ends = count - 1
        head = lax.slice_in_dim(cells, 0, width, axis=dim)
        tail = lax.slice_in_dim(cells, cells.shape[dim] - width, cells.shape[dim], axis=dim)
        cells = jnp.concatenate(
            [
                lax.ppermute(tail, axis, [(i, (i + 1) % count) for i in range(ends)]),
                cells,
                lax.ppermute(head, axis, [((i + 1) % count, i) for i in range(ends)]),
            ],
            axis=dim,
        )
    return cells


def make_projector(gathered, pieces):
    piece_query, piece_key, piece_value, piece_chan = pieces
    joined = jnp.concatenate([piece_key, piece_value], axis=1)
    return (
        jnp.dot(gathered, piece_query, preferred_element_type=jnp.float32),
        jnp.dot(gathered, joined, preferred_element_type=jnp.float32),
        jnp.dot(gathered, piece_chan, preferred_element_type=jnp.float32),
    )


def attend_local(query, keys_ext, sinks, offset, seq_len, key_cols):
    tok_rows, query_cols = query.shape
    kv_local = key_cols // HEAD_DIM
    group = query_cols // key_cols
    block_count = tok_rows // WINDOW
    stacked = keys_ext.reshape(block_count + 2, WINDOW, 2 * key_cols)
    banded = jnp.concatenate([stacked[:-2], stacked[1:-1], stacked[2:]], axis=1)
    key_band = banded[:, :, :key_cols].reshape(block_count, 3 * WINDOW, kv_local, HEAD_DIM)
    value_band = banded[:, :, key_cols:].reshape(block_count, 3 * WINDOW, kv_local, HEAD_DIM)
    query_blocks = query.reshape(block_count, WINDOW, kv_local, group, HEAD_DIM)
    scores = jnp.einsum(
        "nqkgd,nskd->nkgqs", query_blocks, key_band, preferred_element_type=jnp.float32
    ) * HEAD_DIM ** (-0.5)
    starts = offset + jnp.arange(block_count, dtype=jnp.int32) * WINDOW
    query_pos = starts[:, None] + jnp.arange(WINDOW, dtype=jnp.int32)[None, :]
    key_pos = starts[:, None] + jnp.arange(3 * WINDOW, dtype=jnp.int32)[None, :] - WINDOW
    distance = key_pos[:, None, :] - query_pos[:, :, None]
    inside = (key_pos >= 0) & (key_pos < seq_len)
    keep = (jnp.abs(distance) <= WINDOW) & inside[:, None, :]
    scores = jnp.where(keep[:, None, None], scores, masked_score)
    sink_logit = sinks.reshape(kv_local, group)[None, :, :, None, None]
    top = jnp.maximum(jnp.max(scores, axis=-1, keepdims=True), sink_logit)
    raised = jnp.exp(scores - top)
    total = jnp.sum(raised, axis=-1, keepdims=True) + jnp.exp(sink_logit - top)
    probs = (raised / total).astype(jnp.bfloat16)
    attended = jnp.einsum(
        "nkgqs,nskd->nqkgd", probs, value_band, preferred_element_type=jnp.float32
    )
    return attended.astype(jnp.bfloat16).reshape(tok_rows, query_cols)


def local(
    tokens,
    w_query,
    w_key,
    w_value,
    w_pool_in,
    sink,
    w_pool,
    pool_scale,
    w_out_attn,
    w_out_pool,
    out_gain,
):
    tok_rows = tokens.shape[0]
    seq_len = tok_rows * lax.axis_size("sp")
    offset = lax.axis_index("sp") * tok_rows
    out_both = jnp.concatenate([w_out_attn, w_out_pool], axis=0)
    gathered = lax.all_gather(tokens, "tp", axis=1, tiled=True)
    key_cols = w_key.shape[1]
    chan_cols = w_pool_in.shape[1]
    query_sum, joined_sum, chan_sum = make_projector(
        gathered,
        (
            lax.all_gather(w_query, "sp", axis=0, tiled=True),
            lax.all_gather(w_key, "sp", axis=0, tiled=True),
            lax.all_gather(w_value, "sp", axis=0, tiled=True),
            lax.all_gather(w_pool_in, "sp", axis=0, tiled=True),
        ),
    )
    query = query_sum.astype(jnp.bfloat16)
    key_value = joined_sum.astype(jnp.bfloat16)
    chan = chan_sum.astype(jnp.bfloat16)
    keys_ext = padded(key_value, (("sp", 0),), WINDOW)
    attended = attend_local(query, keys_ext, sink, offset, seq_len, key_cols)
    rim_rows = 2 ** (POOL_GROUPS - 1)
    chan_ext = padded(chan, (("sp", 0),), rim_rows)
    running = jnp.concatenate(
        [jnp.zeros((1, chan_cols), jnp.float32), jnp.cumsum(chan_ext.astype(jnp.float32), axis=0)],
        axis=0,
    )
    chan_float = chan.astype(jnp.float32)
    positions = offset + jnp.arange(tok_rows, dtype=jnp.int32)
    group_count = w_pool.shape[0]
    level = lax.axis_index("tp") * group_count + 0
    half = jnp.left_shift(jnp.int32(1), level)
    upper = lax.dynamic_slice_in_dim(running, rim_rows + half, tok_rows, 0)
    lower = lax.dynamic_slice_in_dim(running, rim_rows - half, tok_rows, 0)
    count = (
        jnp.clip(positions + half, 0, seq_len) - jnp.clip(positions - half, 0, seq_len)
    ).astype(jnp.float32)
    spread = ((upper - lower) / count[:, None] - chan_float).astype(jnp.bfloat16)
    outputs = jnp.dot(spread, w_pool[0], preferred_element_type=jnp.float32)
    pooled = (outputs * pool_scale).astype(jnp.bfloat16)
    hidden = jnp.concatenate([attended, pooled], axis=1)
    terms = jnp.dot(
        hidden,
        lax.all_gather(out_both, "sp", axis=1, tiled=True),
        preferred_element_type=jnp.float32,
    )
    share_width = out_gain.shape[0]
    model_width = share_width * lax.axis_size("tp")
    share = lax.psum_scatter(
        terms.astype(jnp.bfloat16), "tp", scatter_dimension=1, tiled=True
    ).astype(jnp.float32)
    row_total, row_square = lax.psum((jnp.sum(share, axis=1), jnp.sum(share * share, axis=1)), "tp")
    row_mean = row_total / model_width
    variance = row_square / model_width - row_mean * row_mean
    normed = (share - row_mean[:, None]) * lax.rsqrt(variance + epsilon)[:, None] * out_gain
    return normed.astype(jnp.bfloat16)


MESH = pl.DeviceIdType.MESH
RIM = 16


def mixer_kernel(
    n,
    tp,
    tok_ref,
    wq_ref,
    wk_ref,
    wv_ref,
    wc_ref,
    sink_ref,
    wp_ref,
    ps_ref,
    woa_ref,
    wop_ref,
    gain_ref,
    out_ref,
    win,
    wout,
    tok,
    acc,
    query,
    kv,
    chan,
    hidden,
    part,
    mated,
    landed,
    own,
    stats,
    win_send,
    win_recv,
    wout_send,
    wout_recv,
    tok_send,
    tok_recv,
    rim_send,
    rim_recv,
    part_send,
    mate_recv,
    part_recv,
    load,
    stat_send,
    stat_recv,
):
    f32, bf16 = jnp.float32, jnp.bfloat16
    me, t = lax.axis_index("sp"), lax.axis_index("tp")
    rows = tok_ref.shape[0]
    seq_len = rows * n
    half_n = n // 2
    column = me % 2
    pos = (me // 2) * (1 - column) + column * (n - 1 - me // 2)

    def at(p):
        p = lax.rem(p + n, n)
        back = p // half_n
        return (1 - back) * (2 * p) + back * (2 * (n - 1 - p) + 1)

    ring = (at(pos + 1), at(pos - 1))
    after, before = lax.rem(me + 1, n), lax.rem(me + n - 1, n)
    mate = t + 1 - 2 * lax.rem(t, 2)
    across = lax.rem(t + 2, tp)
    per = n // tp

    def rdma(src, dst, send, recv, sp, tpi):
        return pltpu.make_async_remote_copy(
            src_ref=src,
            dst_ref=dst,
            send_sem=send,
            recv_sem=recv,
            device_id={"sp": sp, "tp": tpi},
            device_id_type=MESH,
        )

    qc, kc = wq_ref.shape[1], wk_ref.shape[0]
    cc = wc_ref.shape[1]
    depth = wq_ref.shape[0]
    hd = depth // 2
    barrier = pltpu.get_barrier_semaphore()
    peers = [(s, t) for s in ring] + [(s, t) for s in (before, after)]
    peers += [(me, lax.rem(t + i, tp)) for i in range(1, tp)]
    for s, p in peers:
        pl.semaphore_signal(barrier, inc=1, device_id={"sp": s, "tp": p}, device_id_type=MESH)

    loads = []

    def fetch(src, dst):
        copy = pltpu.make_async_copy(src, dst, load.at[len(loads)])
        copy.start()
        loads.append(copy)

    for h in range(2):
        fetch(wq_ref.at[pl.ds(h * hd, hd)], win.at[me, h, :, pl.ds(0, qc)])
        fetch(wc_ref.at[pl.ds(h * hd, hd)], win.at[me, h, :, pl.ds(qc + 2 * kc, cc)])
    for b in range(per):
        fetch(tok_ref.at[:, pl.ds(b * depth, depth)], tok.at[t * per + b])
    fetch(woa_ref, wout.at[me, 0])
    fetch(wop_ref, wout.at[me, 1])
    pair = jnp.transpose(jnp.concatenate([wk_ref[...], wv_ref[...]], axis=0).astype(f32)).astype(bf16)
    for h in range(2):
        win[me, h, :, qc : qc + 2 * kc] = pair[h * hd : (h + 1) * hd]
    for copy in loads:
        copy.wait()
    pl.semaphore_wait(barrier, len(peers))

    def ring_copy(buf, send, recv, way, k, hop):
        sign = -1 if way == 0 else 1
        h = k % 2 if way == 0 else 1 - k % 2
        slot = buf.at[at(pos + sign * (k // 2 + hop)), h]
        return rdma(slot, slot, send.at[way, k], recv.at[way, k], ring[way], t)

    def w_in(way, k, hop):
        return ring_copy(win, win_send, win_recv, way, k, hop)

    def w_out(way, k, hop):
        return ring_copy(wout, wout_send, wout_recv, way, k, hop)

    def tok_copy(owner, b, i, dst):
        slot = tok.at[owner * per + b]
        return rdma(slot, slot, tok_send.at[i], tok_recv.at[i], me, dst)

    for b in range(per):
        tok_copy(t, b, b, across).start()
        for way in range(2):
            if b < 2:
                w_in(way, b, 0).start()
    for b in range(per):
        tok_copy(t, b, per + b, mate).start()

    last = n - 2
    origin = [at(pos)]
    for d in range(1, half_n):
        origin += [at(pos - d), at(pos + d)]
    origin.append(at(pos + half_n))

    def project(i, first=False):
        o = origin[i]
        w = win[o].reshape(depth, qc + 2 * kc + cc)
        term = jnp.dot(tok[o], w, preferred_element_type=f32)
        if first:
            acc[...] = term
        else:
            acc[...] += term

    def relay(copy, k, after_last):
        for way in range(2):
            copy(way, k, 1).wait_recv()
            if k + 2 <= last:
                copy(way, k + 2, 0).start()
            elif after_last is not None:
                after_last(way, k + 1 - last)

    def start_out(way, k):
        w_out(way, k, 0).start()

    ready = 0
    done_blocks = 0
    tok_step = {1: 0, 3: 1}
    tokens_here = False
    for k in range(last + 1):
        relay(w_in, k, start_out)
        if k in tok_step:
            b = tok_step[k]
            tok_copy(across, b, b, across).wait_recv()
            tok_copy(across, b, 2 * per + b, mate).start()
        if k == 3:
            for b in range(per):
                tok_copy(mate, b, per + b, mate).wait_recv()
                tok_copy(lax.rem(mate + 2, tp), b, 2 * per + b, mate).wait_recv()
            tokens_here = True
        ready = 1 + 2 * ((k + 1) // 2) if k < last else n
        if tokens_here:
            while done_blocks < ready and (k == last or done_blocks < 1 + 2 * ((k - 2) // 1)):
                project(done_blocks, done_blocks == 0)
                done_blocks += 1

    query[...] = acc[:, 0:qc].astype(bf16)
    kv[WINDOW : WINDOW + rows, :] = acc[:, qc : qc + 2 * kc].astype(bf16)
    chan[RIM : RIM + rows, :] = acc[:, qc + 2 * kc :].astype(bf16)

    def rim(buf, width, down, i):
        if down:
            return rdma(buf.at[pl.ds(rows, width)], buf.at[pl.ds(0, width)], rim_send.at[i], rim_recv.at[i], after, t)
        return rdma(
            buf.at[pl.ds(width, width)], buf.at[pl.ds(rows + width, width)], rim_send.at[i], rim_recv.at[i], before, t
        )

    rims = [rim(kv, WINDOW, True, 0), rim(kv, WINDOW, False, 1), rim(chan, RIM, True, 2), rim(chan, RIM, False, 3)]
    for c in rims:
        c.start()

    group = qc // kc

    def attend(b):
        band = kv[b * WINDOW : (b + 3) * WINDOW, :]
        q = query[b * WINDOW : (b + 1) * WINDOW, :]
        stacked = jnp.concatenate([q[:, g * HEAD_DIM : (g + 1) * HEAD_DIM] for g in range(group)], axis=0)
        scores = lax.dot_general(
            stacked, band[:, :HEAD_DIM], (((1,), (1,)), ((), ())), preferred_element_type=f32
        ) * HEAD_DIM ** (-0.5)
        scores = scores.reshape(group, WINDOW, 3 * WINDOW)
        r = lax.broadcasted_iota(jnp.int32, (WINDOW, 3 * WINDOW), 0)
        c = lax.broadcasted_iota(jnp.int32, (WINDOW, 3 * WINDOW), 1)
        keep = (c >= r) & (c <= r + 2 * WINDOW)
        key_pos = c + (me * rows + b * WINDOW - WINDOW)
        keep = keep & (key_pos >= 0) & (key_pos < seq_len)
        outs = []
        for g in range(group):
            s = jnp.where(keep, scores[g], masked_score)
            logit = sink_ref[0, g]
            top = jnp.maximum(jnp.max(s, axis=1, keepdims=True), logit)
            raised = jnp.exp(s - top)
            total = jnp.sum(raised, axis=1, keepdims=True) + jnp.exp(logit - top)
            outs.append((raised * (1.0 / total)).astype(bf16))
        got = jnp.dot(jnp.concatenate(outs, axis=0), band, preferred_element_type=f32)
        got = got[:, HEAD_DIM : 2 * HEAD_DIM].astype(bf16)
        hidden[b * WINDOW : (b + 1) * WINDOW, 0:qc] = jnp.concatenate(
            [got[g * WINDOW : (g + 1) * WINDOW] for g in range(group)], axis=1
        )

    def pool():
        length = rows + 2 * RIM
        e = chan[...].astype(f32)
        p = lax.broadcasted_iota(jnp.int32, (length, 1), 0) + (me * rows - RIM)
        e = jnp.where((p >= 0) & (p < seq_len), e, 0.0)
        sums = e + pltpu.roll(e, 1, 0)
        pick = sums
        for level in range(1, POOL_GROUPS):
            step = 2 ** (level - 1)
            sums = pltpu.roll(sums, step, 0) + pltpu.roll(sums, length - step, 0)
            pick = jnp.where(t == level, sums, pick)
        half = 1
        for level in range(1, POOL_GROUPS):
            half = jnp.where(t == level, 2**level, half)
        count = (jnp.clip(p + half, 0, seq_len) - jnp.clip(p - half, 0, seq_len)).astype(f32)
        spread = (pick[RIM : RIM + rows] / count[RIM : RIM + rows] - e[RIM : RIM + rows]).astype(bf16)
        got = jnp.dot(spread, wp_ref[0], preferred_element_type=f32)
        hidden[:, qc:] = (got * ps_ref[...]).astype(bf16)

    def to_mate(o):
        return rdma(part.at[o], mated.at[o], part_send.at[o], mate_recv.at[o], me, mate)

    def to_owner(o):
        s = lax.rem(o, per)
        return rdma(part.at[o], landed.at[s], part_send.at[o], part_recv.at[s], me, across)

    def emit(i):
        o = origin[i]
        got = jnp.dot(hidden[:, 0:qc], wout[o, 0], preferred_element_type=f32)
        got = got + jnp.dot(hidden[:, qc:], wout[o, 1], preferred_element_type=f32)
        part[o] = got.astype(bf16)

        @pl.when(lax.rem(o // per, 2) != lax.rem(t, 2))
        def _():
            to_mate(o).start()

    def combine(i):
        o = origin[i]

        @pl.when(o // per == t)
        def _():
            to_mate(o).wait_recv()
            own[lax.rem(o, per)] = part[o].astype(f32) + mated[o].astype(f32)

        @pl.when(o // per == across)
        def _():
            to_mate(o).wait_recv()
            part[o] = (part[o].astype(f32) + mated[o].astype(f32)).astype(bf16)
            to_owner(o).start()

    blocks = rows // WINDOW
    relay(w_out, 0, None)
    for b in range(1, blocks - 1):
        attend(b)
    relay(w_out, 1, None)
    for c in rims:
        c.wait()
    pool()
    relay(w_out, 2, None)
    attend(0)
    relay(w_out, 3, None)
    attend(blocks - 1)
    for i in range(0, 5):
        emit(i)
    for i in range(0, 5):
        combine(i)
    for k in range(4, last + 1):
        relay(w_out, k, None)
        if k % 2 == 1:
            emit(k)
            emit(k + 1)
            combine(k)
            combine(k + 1)
    emit(n - 1)
    combine(n - 1)

    share = []
    for s in range(per):
        to_owner(t * per + s).wait_recv()
        share.append(own[s] + landed[s].astype(f32))
    mix = jnp.concatenate(share, axis=1)
    acc[:, 0 : mix.shape[1]] = mix
    one = jnp.sum(mix, axis=1, keepdims=True)
    two = jnp.sum(mix * mix, axis=1, keepdims=True)
    lane = lax.broadcasted_iota(jnp.int32, (rows, 128), 1)
    both = jnp.where(lane == 0, one, jnp.where(lane == 1, two, 0.0))
    stats[t] = jnp.transpose(both)[0:8]

    def stat_copy(j):
        return rdma(stats.at[t], stats.at[t], stat_send.at[j], stat_recv.at[t], me, lax.rem(t + j, tp))

    for j in range(1, tp):
        stat_copy(j).start()
    for o in range(n):

        @pl.when(o // per != t)
        def _():
            to_mate(o).wait_send()

    for k in range(last + 1):
        for way in range(2):
            w_in(way, k, 0).wait_send()
            w_out(way, k, 0).wait_send()
    for b in range(per):
        tok_copy(t, b, b, across).wait_send()
        tok_copy(t, b, per + b, mate).wait_send()
        tok_copy(across, b, 2 * per + b, mate).wait_send()
    for j in range(1, tp):
        src = lax.rem(t + j, tp)
        rdma(stats.at[src], stats.at[src], stat_send.at[j], stat_recv.at[src], me, src).wait_recv()
    totals = stats[0]
    for i in range(1, tp):
        totals = totals + stats[i]
    wide = jnp.concatenate([totals, jnp.zeros((120, rows), f32)], axis=0)
    back = jnp.transpose(wide)
    width = gain_ref.shape[1] * tp
    row_mean = back[:, 0:1] / width
    variance = back[:, 1:2] / width - row_mean * row_mean
    scale = lax.rsqrt(variance + epsilon)
    out_ref[...] = ((acc[:, 0 : gain_ref.shape[1]] - row_mean) * scale * gain_ref[...]).astype(bf16)
    for j in range(1, tp):
        stat_copy(j).wait_send()


def fused(n, tp, tokens, w_query, w_key, w_value, w_pool_in, sink, w_pool, pool_scale, w_out_attn, w_out_pool, out_gain):
    rows, share = tokens.shape
    depth, qc = w_query.shape
    kc, cc = w_key.shape[1], w_pool_in.shape[1]
    wide = w_out_attn.shape[1]
    per = n // tp
    bf16, f32 = jnp.bfloat16, jnp.float32
    dma = pltpu.SemaphoreType.DMA
    vmem = pl.BlockSpec(memory_space=pltpu.VMEM)
    specs = [vmem] * 11
    specs[5] = pl.BlockSpec(memory_space=pltpu.SMEM)
    for i in (0, 1, 4, 8, 9):
        specs[i] = pl.BlockSpec(memory_space=pl.ANY)
    return pl.pallas_call(
        functools.partial(mixer_kernel, n, tp),
        out_shape=jax.ShapeDtypeStruct((rows, share), bf16),
        in_specs=specs,
        out_specs=vmem,
        scratch_shapes=[
            pltpu.VMEM((n, 2, depth // 2, qc + 2 * kc + cc), bf16),
            pltpu.VMEM((n, 2, qc, wide), bf16),
            pltpu.VMEM((n, rows, depth), bf16),
            pltpu.VMEM((rows, qc + 2 * kc + cc), f32),
            pltpu.VMEM((rows, qc), bf16),
            pltpu.VMEM((rows + 2 * WINDOW, 2 * kc), bf16),
            pltpu.VMEM((rows + 2 * RIM, cc), bf16),
            pltpu.VMEM((rows, qc + cc), bf16),
            pltpu.VMEM((n, rows, wide), bf16),
            pltpu.VMEM((n, rows, wide), bf16),
            pltpu.VMEM((per, rows, wide), bf16),
            pltpu.VMEM((per, rows, wide), f32),
            pltpu.VMEM((tp, 8, rows), f32),
            dma((2, n - 1)),
            dma((2, n - 1)),
            dma((2, n - 1)),
            dma((2, n - 1)),
            dma((3 * per,)),
            dma((3 * per,)),
            dma((4,)),
            dma((4,)),
            dma((n,)),
            dma((n,)),
            dma((per,)),
            dma((6 + per,)),
            dma((tp,)),
            dma((tp,)),
        ],
        compiler_params=pltpu.CompilerParams(
            collective_id=0, has_side_effects=True, vmem_limit_bytes=60 * 1024 * 1024
        ),
        name="mixer",
    )(
        tokens,
        w_query,
        w_key.T,
        w_value.T,
        w_pool_in,
        sink.reshape(1, -1),
        w_pool,
        pool_scale.reshape(1, -1),
        w_out_attn,
        w_out_pool,
        out_gain.reshape(1, -1),
    )


def fits(n, tp, tokens, w_query, w_key, w_pool, w_out_attn):
    return (
        tp == 4
        and n == 2 * tp
        and w_query.shape[0] % 32 == 0
        and w_query.shape[1] % 128 == 0
        and w_key.shape[1] == HEAD_DIM
        and w_pool.shape[0] == 1
        and w_out_attn.shape[1] % 128 == 0
        and tokens.shape[0] >= 2 * WINDOW
    )


def mixed_rows(*args):
    n, tp = lax.axis_size("sp"), lax.axis_size("tp")
    if fits(n, tp, args[0], args[1], args[2], args[6], args[8]):
        return fused(n, tp, *args)
    return local(*args)


def solution(mesh):
    return jax.shard_map(
        mixed_rows,
        mesh=mesh,
        in_specs=(
            P("sp", "tp"),
            P("sp", "tp"),
            P("sp", "tp"),
            P("sp", "tp"),
            P("sp", "tp"),
            P("tp"),
            P("tp", None, None),
            P("tp"),
            P("tp", "sp"),
            P("tp", "sp"),
            P("tp"),
        ),
        out_specs=P("sp", "tp"),
        check_vma=False,
    )
```

profile of v0, /device:TPU:0, one launch (start us, length us, event | category | flops | bytes accessed | tf_op | source)
XLA Modules:
  0.0 68.4 jit_solution(13605473591724609113)
XLA Ops:
  0.0 66.5 %mixer.1 = bf16[512,512]{1,0:T(8,128)(2,1)} custom-call(bf16[512,512]{1,0:T(8,128)(2,1)} %tok_ref.1, bf16[256,256]{1,0:T(8,128)(2,1)} %wq_ref.1, bf16[64,256]{1,0:T(8,128)(2,1)} %bitcast.5, bf16[64,256]{1,0:T(8,128)(2,1)} %bitcast.6, bf16[256,256]{1,0:T(8,128)(2,1)} %wc_ref.1, f32[1,4]{1,0:T(1,128)} %bitcast.9, bf16[1,256,256]{2,1,0:T(8,128)(2,1)} %wp_ref.1, ...), custom_call_target="tpu_custom_call" | custom-call | tf_op jit(solution)/shard_map/mixer/pallas_call | solution.py:507
  66.5 1.9 %copy.13 = bf16[512,512]{1,0:T(8,128)(2,1)} copy(bf16[512,512]{1,0:T(8,128)(2,1)} %mixer.1) | data formatting | bytes 1048576
where the time goes:
time: 69.3 us; the launch traced here: 68.4 us
  Pallas kernels  66.5 us (96%)
  local copies, waits for them, and re-layouts  1.87 us (3%)
    pallas_call x1, Pallas kernels, fused(): pl.pallas_call(functools.partial(mixer_kernel, n, tp), out_shape=jax.Shap...  66.5 us
    unnamed x1, local copies, waits for them, and re-layouts  1.87 us

commit v1 on v0

--- a/solution.py
+++ b/solution.py
@@ -147,6 +147,7 @@
 
 MESH = pl.DeviceIdType.MESH
 RIM = 16
+QUARTERS = 4
 
 
 def mixer_kernel(
@@ -177,6 +178,11 @@
     landed,
     own,
     stats,
+    pair_in,
+    sinks,
+    wpool,
+    scales,
+    gains,
     win_send,
     win_recv,
     wout_send,
@@ -224,7 +230,9 @@
     qc, kc = wq_ref.shape[1], wk_ref.shape[0]
     cc = wc_ref.shape[1]
     depth = wq_ref.shape[0]
-    hd = depth // 2
+    quarter = depth // QUARTERS
+    wide = woa_ref.shape[1]
+    half = wide // 2
     barrier = pltpu.get_barrier_semaphore()
     peers = [(s, t) for s in ring] + [(s, t) for s in (before, after)]
     peers += [(me, lax.rem(t + i, tp)) for i in range(1, tp)]
@@ -237,25 +245,37 @@
         copy = pltpu.make_async_copy(src, dst, load.at[len(loads)])
         copy.start()
         loads.append(copy)
-
+        return copy
+
+    pairs = [fetch(wk_ref, pair_in.at[pl.ds(0, kc)]), fetch(wv_ref, pair_in.at[pl.ds(kc, kc)])]
+    first = []
+    for h in range(QUARTERS):
+        rows_in = pl.ds(h * quarter, quarter)
+        first.append(fetch(wq_ref.at[rows_in], win.at[me, h, :, pl.ds(0, qc)]))
+        first.append(fetch(wc_ref.at[rows_in], win.at[me, h, :, pl.ds(qc + 2 * kc, cc)]))
+    own_tok = [fetch(tok_ref.at[:, pl.ds(b * depth, depth)], tok.at[t * per + b]) for b in range(per)]
+    later = []
     for h in range(2):
-        fetch(wq_ref.at[pl.ds(h * hd, hd)], win.at[me, h, :, pl.ds(0, qc)])
-        fetch(wc_ref.at[pl.ds(h * hd, hd)], win.at[me, h, :, pl.ds(qc + 2 * kc, cc)])
-    for b in range(per):
-        fetch(tok_ref.at[:, pl.ds(b * depth, depth)], tok.at[t * per + b])
-    fetch(woa_ref, wout.at[me, 0])
-    fetch(wop_ref, wout.at[me, 1])
-    pair = jnp.transpose(jnp.concatenate([wk_ref[...], wv_ref[...]], axis=0).astype(f32)).astype(bf16)
-    for h in range(2):
-        win[me, h, :, qc : qc + 2 * kc] = pair[h * hd : (h + 1) * hd]
-    for copy in loads:
+        later.append(fetch(woa_ref.at[:, pl.ds(h * half, half)], wout.at[me, h, 0]))
+        later.append(fetch(wop_ref.at[:, pl.ds(h * half, half)], wout.at[me, h, 1]))
+    later.append(fetch(sink_ref, sinks))
+    later.append(fetch(wp_ref, wpool))
+    later.append(fetch(ps_ref, scales))
+    later.append(fetch(gain_ref, gains))
+    for copy in pairs:
+        copy.wait()
+    pair = jnp.transpose(pair_in[...].astype(f32)).astype(bf16)
+    for h in range(QUARTERS):
+        win[me, h, :, qc : qc + 2 * kc] = pair[h * quarter : (h + 1) * quarter]
+    for copy in first:
         copy.wait()
     pl.semaphore_wait(barrier, len(peers))
 
     def ring_copy(buf, send, recv, way, k, hop):
         sign = -1 if way == 0 else 1
-        h = k % 2 if way == 0 else 1 - k % 2
-        slot = buf.at[at(pos + sign * (k // 2 + hop)), h]
+        q = k % QUARTERS if way == 0 else QUARTERS - 1 - k % QUARTERS
+        o = at(pos + sign * (k // QUARTERS + hop))
+        slot = buf.at[o, q] if buf is win else buf.at[o, q // 2, q % 2]
         return rdma(slot, slot, send.at[way, k], recv.at[way, k], ring[way], t)
 
     def w_in(way, k, hop):
@@ -268,15 +288,20 @@
         slot = tok.at[owner * per + b]
         return rdma(slot, slot, tok_send.at[i], tok_recv.at[i], me, dst)
 
+    count = QUARTERS * (n - 1) // 2
+    last = count - 1
+    for k in range(QUARTERS):
+        for way in range(2):
+            w_in(way, k, 0).start()
+    for copy in own_tok:
+        copy.wait()
     for b in range(per):
         tok_copy(t, b, b, across).start()
-        for way in range(2):
-            if b < 2:
-                w_in(way, b, 0).start()
     for b in range(per):
         tok_copy(t, b, per + b, mate).start()
-
-    last = n - 2
+    for copy in later:
+        copy.wait()
+
     origin = [at(pos)]
     for d in range(1, half_n):
         origin += [at(pos - d), at(pos + d)]
@@ -291,39 +316,36 @@
         else:
             acc[...] += term
 
-    def relay(copy, k, after_last):
+    def relay(copy, k):
         for way in range(2):
             copy(way, k, 1).wait_recv()
-            if k + 2 <= last:
-                copy(way, k + 2, 0).start()
-            elif after_last is not None:
-                after_last(way, k + 1 - last)
-
-    def start_out(way, k):
-        w_out(way, k, 0).start()
-
-    ready = 0
+            if k + QUARTERS <= last:
+                copy(way, k + QUARTERS, 0).start()
+
+    def start_out(k):
+        for way in range(2):
+            w_out(way, k, 0).start()
+
     done_blocks = 0
-    tok_step = {1: 0, 3: 1}
-    tokens_here = False
-    for k in range(last + 1):
-        relay(w_in, k, start_out)
-        if k in tok_step:
-            b = tok_step[k]
+    for k in range(count):
+        relay(w_in, k)
+        if k in (last - 3, last - 2):
+            start_out(k - (last - 3))
+        if k in (3, 6):
+            b = 0 if k == 3 else 1
             tok_copy(across, b, b, across).wait_recv()
             tok_copy(across, b, 2 * per + b, mate).start()
-        if k == 3:
+        if k == 8:
             for b in range(per):
                 tok_copy(mate, b, per + b, mate).wait_recv()
                 tok_copy(lax.rem(mate + 2, tp), b, 2 * per + b, mate).wait_recv()
-            tokens_here = True
-        ready = 1 + 2 * ((k + 1) // 2) if k < last else n
-        if tokens_here:
-            while done_blocks < ready and (k == last or done_blocks < 1 + 2 * ((k - 2) // 1)):
+        if k >= 8:
+            ready = n if k == last else 1 + 2 * ((k + 1) // QUARTERS)
+            upto = ready if k == last else min(ready, done_blocks + 2)
+            while done_blocks < upto:
                 project(done_blocks, done_blocks == 0)
                 done_blocks += 1
 
-    query[...] = acc[:, 0:qc].astype(bf16)
     kv[WINDOW : WINDOW + rows, :] = acc[:, qc : qc + 2 * kc].astype(bf16)
     chan[RIM : RIM + rows, :] = acc[:, qc + 2 * kc :].astype(bf16)
 
@@ -337,6 +359,9 @@
     rims = [rim(kv, WINDOW, True, 0), rim(kv, WINDOW, False, 1), rim(chan, RIM, True, 2), rim(chan, RIM, False, 3)]
     for c in rims:
         c.start()
+    start_out(2)
+    start_out(3)
+    query[...] = acc[:, 0:qc].astype(bf16)
 
     group = qc // kc
 
@@ -356,7 +381,7 @@
         outs = []
         for g in range(group):
             s = jnp.where(keep, scores[g], masked_score)
-            logit = sink_ref[0, g]
+            logit = sinks[0:1, g : g + 1]
             top = jnp.maximum(jnp.max(s, axis=1, keepdims=True), logit)
             raised = jnp.exp(s - top)
             total = jnp.sum(raised, axis=1, keepdims=True) + jnp.exp(logit - top)
@@ -378,75 +403,81 @@
             step = 2 ** (level - 1)
             sums = pltpu.roll(sums, step, 0) + pltpu.roll(sums, length - step, 0)
             pick = jnp.where(t == level, sums, pick)
-        half = 1
+        half_width = 1
         for level in range(1, POOL_GROUPS):
-            half = jnp.where(t == level, 2**level, half)
-        count = (jnp.clip(p + half, 0, seq_len) - jnp.clip(p - half, 0, seq_len)).astype(f32)
-        spread = (pick[RIM : RIM + rows] / count[RIM : RIM + rows] - e[RIM : RIM + rows]).astype(bf16)
-        got = jnp.dot(spread, wp_ref[0], preferred_element_type=f32)
-        hidden[:, qc:] = (got * ps_ref[...]).astype(bf16)
-
-    def to_mate(o):
-        return rdma(part.at[o], mated.at[o], part_send.at[o], mate_recv.at[o], me, mate)
-
-    def to_owner(o):
+            half_width = jnp.where(t == level, 2**level, half_width)
+        number = (jnp.clip(p + half_width, 0, seq_len) - jnp.clip(p - half_width, 0, seq_len)).astype(f32)
+        spread = (pick[RIM : RIM + rows] / number[RIM : RIM + rows] - e[RIM : RIM + rows]).astype(bf16)
+        got = jnp.dot(spread, wpool[0], preferred_element_type=f32)
+        hidden[:, qc:] = (got * scales[...]).astype(bf16)
+
+    def to_mate(o, h):
+        return rdma(part.at[o, h], mated.at[o, h], part_send.at[o, h], mate_recv.at[o, h], me, mate)
+
+    def to_owner(o, h):
         s = lax.rem(o, per)
-        return rdma(part.at[o], landed.at[s], part_send.at[o], part_recv.at[s], me, across)
+        return rdma(part.at[o, h], landed.at[s, h], part_send.at[o, h], part_recv.at[s, h], me, across)
+
+    pieces = [(0, 0), (0, 1)]
+    for k in range(1, count, 2):
+        d, h = k // QUARTERS, (k % QUARTERS) // 2
+        pieces += [(min(2 * d + 1, n - 1), h), (min(2 * d + 2, n - 1), 1 - h)]
 
     def emit(i):
-        o = origin[i]
-        got = jnp.dot(hidden[:, 0:qc], wout[o, 0], preferred_element_type=f32)
-        got = got + jnp.dot(hidden[:, qc:], wout[o, 1], preferred_element_type=f32)
-        part[o] = got.astype(bf16)
+        o, h = origin[pieces[i][0]], pieces[i][1]
+        got = jnp.dot(hidden[...], wout[o, h].reshape(qc + cc, half), preferred_element_type=f32)
+        part[o, h] = got.astype(bf16)
 
         @pl.when(lax.rem(o // per, 2) != lax.rem(t, 2))
         def _():
-            to_mate(o).start()
+            to_mate(o, h).start()
 
     def combine(i):
-        o = origin[i]
+        o, h = origin[pieces[i][0]], pieces[i][1]
 
         @pl.when(o // per == t)
         def _():
-            to_mate(o).wait_recv()
-            own[lax.rem(o, per)] = part[o].astype(f32) + mated[o].astype(f32)
+            to_mate(o, h).wait_recv()
+            own[lax.rem(o, per), h] = part[o, h].astype(f32) + mated[o, h].astype(f32)
 
         @pl.when(o // per == across)
         def _():
-            to_mate(o).wait_recv()
-            part[o] = (part[o].astype(f32) + mated[o].astype(f32)).astype(bf16)
-            to_owner(o).start()
+            to_mate(o, h).wait_recv()
+            part[o, h] = (part[o, h].astype(f32) + mated[o, h].astype(f32)).astype(bf16)
+            to_owner(o, h).start()
 
     blocks = rows // WINDOW
-    relay(w_out, 0, None)
-    for b in range(1, blocks - 1):
-        attend(b)
-    relay(w_out, 1, None)
-    for c in rims:
-        c.wait()
-    pool()
-    relay(w_out, 2, None)
-    attend(0)
-    relay(w_out, 3, None)
-    attend(blocks - 1)
-    for i in range(0, 5):
-        emit(i)
-    for i in range(0, 5):
-        combine(i)
-    for k in range(4, last + 1):
-        relay(w_out, k, None)
-        if k % 2 == 1:
-            emit(k)
-            emit(k + 1)
-            combine(k)
-            combine(k + 1)
-    emit(n - 1)
-    combine(n - 1)
+    inner = list(range(1, blocks - 1))
+    emitted = combined = 0
+    for k in range(count):
+        relay(w_out, k)
+        if k < 2:
+            for b in inner[k :: 2]:
+                attend(b)
+        elif k == 2:
+            for c in rims:
+                c.wait()
+            attend(0)
+        elif k == 3:
+            attend(blocks - 1)
+        elif k == 4:
+            pool()
+        else:
+            here = 2 + 2 * ((k + 1) // 2)
+            goal = here if k == last else min(here, emitted + 3)
+            behind = emitted
+            while emitted < goal:
+                emit(emitted)
+                emitted += 1
+            while combined < (emitted if k == last else behind):
+                combine(combined)
+                combined += 1
 
     share = []
     for s in range(per):
-        to_owner(t * per + s).wait_recv()
-        share.append(own[s] + landed[s].astype(f32))
+        for h in range(2):
+            to_owner(t * per + s, h).wait_recv()
+            share.append(own[s, h] + landed[s, h].astype(f32))
     mix = jnp.concatenate(share, axis=1)
     acc[:, 0 : mix.shape[1]] = mix
     one = jnp.sum(mix, axis=1, keepdims=True)
@@ -464,9 +495,10 @@
 
         @pl.when(o // per != t)
         def _():
-            to_mate(o).wait_send()
-
-    for k in range(last + 1):
+            for h in range(2):
+                to_mate(o, h).wait_send()
+
+    for k in range(count):
         for way in range(2):
             w_in(way, k, 0).wait_send()
             w_out(way, k, 0).wait_send()
@@ -480,13 +512,13 @@
     totals = stats[0]
     for i in range(1, tp):
         totals = totals + stats[i]
-    wide = jnp.concatenate([totals, jnp.zeros((120, rows), f32)], axis=0)
-    back = jnp.transpose(wide)
+    tall = jnp.concatenate([totals, jnp.zeros((120, rows), f32)], axis=0)
+    back = jnp.transpose(tall)
     width = gain_ref.shape[1] * tp
     row_mean = back[:, 0:1] / width
     variance = back[:, 1:2] / width - row_mean * row_mean
     scale = lax.rsqrt(variance + epsilon)
-    out_ref[...] = ((acc[:, 0 : gain_ref.shape[1]] - row_mean) * scale * gain_ref[...]).astype(bf16)
+    out_ref[...] = ((acc[:, 0 : gain_ref.shape[1]] - row_mean) * scale * gains[...]).astype(bf16)
     for j in range(1, tp):
         stat_copy(j).wait_send()
 
@@ -496,64 +528,66 @@
     depth, qc = w_query.shape
     kc, cc = w_key.shape[1], w_pool_in.shape[1]
     wide = w_out_attn.shape[1]
+    half = wide // 2
     per = n // tp
+    count = QUARTERS * (n - 1) // 2
     bf16, f32 = jnp.bfloat16, jnp.float32
     dma = pltpu.SemaphoreType.DMA
-    vmem = pl.BlockSpec(memory_space=pltpu.VMEM)
-    specs = [vmem] * 11
-    specs[5] = pl.BlockSpec(memory_space=pltpu.SMEM)
-    for i in (0, 1, 4, 8, 9):
-        specs[i] = pl.BlockSpec(memory_space=pl.ANY)
     return pl.pallas_call(
         functools.partial(mixer_kernel, n, tp),
         out_shape=jax.ShapeDtypeStruct((rows, share), bf16),
-        in_specs=specs,
-        out_specs=vmem,
+        in_specs=[pl.BlockSpec(memory_space=pltpu.HBM)] * 11,
+        out_specs=pl.BlockSpec(memory_space=pltpu.VMEM),
         scratch_shapes=[
-            pltpu.VMEM((n, 2, depth // 2, qc + 2 * kc + cc), bf16),
-            pltpu.VMEM((n, 2, qc, wide), bf16),
+            pltpu.VMEM((n, QUARTERS, depth // QUARTERS, qc + 2 * kc + cc), bf16),
+            pltpu.VMEM((n, 2, 2, qc, half), bf16),
             pltpu.VMEM((n, rows, depth), bf16),
             pltpu.VMEM((rows, qc + 2 * kc + cc), f32),
             pltpu.VMEM((rows, qc), bf16),
             pltpu.VMEM((rows + 2 * WINDOW, 2 * kc), bf16),
             pltpu.VMEM((rows + 2 * RIM, cc), bf16),
             pltpu.VMEM((rows, qc + cc), bf16),
-            pltpu.VMEM((n, rows, wide), bf16),
-            pltpu.VMEM((n, rows, wide), bf16),
-            pltpu.VMEM((per, rows, wide), bf16),
-            pltpu.VMEM((per, rows, wide), f32),
+            pltpu.VMEM((n, 2, rows, half), bf16),
+            pltpu.VMEM((n, 2, rows, half), bf16),
+            pltpu.VMEM((per, 2, rows, half), bf16),
+            pltpu.VMEM((per, 2, rows, half), f32),
             pltpu.VMEM((tp, 8, rows), f32),
-            dma((2, n - 1)),
-            dma((2, n - 1)),
-            dma((2, n - 1)),
-            dma((2, n - 1)),
+            pltpu.VMEM((2 * kc, depth), bf16),
+            pltpu.VMEM((1, sink.shape[0]), f32),
+            pltpu.VMEM(w_pool.shape, bf16),
+            pltpu.VMEM((1, cc), f32),
+            pltpu.VMEM((1, share), f32),
+            dma((2, count)),
+            dma((2, count)),
+            dma((2, count)),
+            dma((2, count)),
             dma((3 * per,)),
             dma((3 * per,)),
             dma((4,)),
             dma((4,)),
-            dma((n,)),
-            dma((n,)),
-            dma((per,)),
-            dma((6 + per,)),
+            dma((n, 2)),
+            dma((n, 2)),
+            dma((per, 2)),
+            dma((2 * QUARTERS + per + 10,)),
             dma((tp,)),
             dma((tp,)),
         ],
         compiler_params=pltpu.CompilerParams(
-            collective_id=0, has_side_effects=True, vmem_limit_bytes=60 * 1024 * 1024
+            collective_id=0, has_side_effects=True, vmem_limit_bytes=32 * 1024 * 1024
         ),
         name="mixer",
     )(
-        tokens,
-        w_query,
-        w_key.T,
-        w_value.T,
-        w_pool_in,
-        sink.reshape(1, -1),
-        w_pool,
-        pool_scale.reshape(1, -1),
-        w_out_attn,
-        w_out_pool,
-        out_gain.reshape(1, -1),
+        pltpu.with_memory_space_constraint(tokens, pltpu.HBM),
+        pltpu.with_memory_space_constraint(w_query, pltpu.HBM),
+        pltpu.with_memory_space_constraint(w_key.T, pltpu.HBM),
+        pltpu.with_memory_space_constraint(w_value.T, pltpu.HBM),
+        pltpu.with_memory_space_constraint(w_pool_in, pltpu.HBM),
+        pltpu.with_memory_space_constraint(sink.reshape(1, -1), pltpu.HBM),
+        pltpu.with_memory_space_constraint(w_pool, pltpu.HBM),
+        pltpu.with_memory_space_constraint(pool_scale.reshape(1, -1), pltpu.HBM),
+        pltpu.with_memory_space_constraint(w_out_attn, pltpu.HBM),
+        pltpu.with_memory_space_constraint(w_out_pool, pltpu.HBM),
+        pltpu.with_memory_space_constraint(out_gain.reshape(1, -1), pltpu.HBM),
     )
 
 
@@ -561,11 +595,12 @@
     return (
         tp == 4
         and n == 2 * tp
-        and w_query.shape[0] % 32 == 0
+        and w_query.shape[0] % 64 == 0
         and w_query.shape[1] % 128 == 0
         and w_key.shape[1] == HEAD_DIM
         and w_pool.shape[0] == 1
-        and w_out_attn.shape[1] % 128 == 0
+        and w_out_attn.shape[1] % 256 == 0
+        and w_out_attn.shape[0] == w_query.shape[1]
         and tokens.shape[0] >= 2 * WINDOW
     )
 

time: 69.3 us -> 66.3 us (0.957); the launches traced: 68.4 us -> 66.2 us
  Pallas kernels: 66.5 us -> 65.4 us
  local copies, waits for them, and re-layouts: 1.87 us -> 0.8 us
    pallas_call x1, Pallas kernels: 66.5 us -> 65.4 us  [fused(): pl.pallas_call(functools.partial(mixer_kernel, n, tp), out_shape=jax.Shap...]
    unnamed x1, local copies, waits for them, and re-layouts: 1.87 us -> 0.8 us
where the time goes in v1:
time: 66.3 us; the launch traced here: 66.2 us
  Pallas kernels  65.4 us (99%)
  local copies, waits for them, and re-layouts  0.8 us (1%)
    pallas_call x1, Pallas kernels, fused(): pl.pallas_call(functools.partial(mixer_kernel, n, tp), out_shape=jax.Shap...  65.4 us

profile of v1, /device:TPU:0, one launch (start us, length us, event | category | flops | bytes accessed | tf_op | source)
XLA Modules:
  0.0 66.2 jit_solution(2264806125463764977)
XLA Ops:
  0.0 65.4 %mixer.1 = bf16[512,512]{1,0:T(8,128)(2,1)S(1)} custom-call(bf16[512,512]{1,0:T(8,128)(2,1)} %tok_ref.1, bf16[256,256]{1,0:T(8,128)(2,1)} %wq_ref.1, bf16[64,256]{1,0:T(8,128)(2,1)} %bitcast.5, bf16[64,256]{1,0:T(8,128)(2,1)} %bitcast.6, bf16[256,256]{1,0:T(8,128)(2,1)} %wc_ref.1, f32[1,4]{1,0:T(1,128)} %bitcast.9, bf16[1,256,256]{2,1,0:T(8,128)(2,1)} %wp_ref.1, ...), custom_call_target="tpu_custom_call" | custom-call | tf_op jit(solution)/shard_map/mixer/pallas_call | solution.py:536
  65.4 0.8 %copy.13 = bf16[512,512]{1,0:T(8,128)(2,1)} copy(bf16[512,512]{1,0:T(8,128)(2,1)S(1)} %mixer.1) | data formatting | bytes 1048576

commit v2 on v1

--- a/solution.py
+++ b/solution.py
@@ -148,6 +148,7 @@
 MESH = pl.DeviceIdType.MESH
 RIM = 16
 QUARTERS = 4
+SENDS = 8
 
 
 def mixer_kernel(
@@ -183,10 +184,8 @@
     wpool,
     scales,
     gains,
-    win_send,
-    win_recv,
-    wout_send,
-    wout_recv,
+    ring_send,
+    ring_recv,
     tok_send,
     tok_recv,
     rim_send,
@@ -227,9 +226,9 @@
             device_id_type=MESH,
         )
 
-    qc, kc = wq_ref.shape[1], wk_ref.shape[0]
-    cc = wc_ref.shape[1]
-    depth = wq_ref.shape[0]
+    qc, kc = wq_ref.shape[2], wk_ref.shape[0]
+    cc = wc_ref.shape[2]
+    depth = QUARTERS * wq_ref.shape[1]
     quarter = depth // QUARTERS
     wide = woa_ref.shape[1]
     half = wide // 2
@@ -248,11 +247,10 @@
         return copy
 
     pairs = [fetch(wk_ref, pair_in.at[pl.ds(0, kc)]), fetch(wv_ref, pair_in.at[pl.ds(kc, kc)])]
-    first = []
-    for h in range(QUARTERS):
-        rows_in = pl.ds(h * quarter, quarter)
-        first.append(fetch(wq_ref.at[rows_in], win.at[me, h, :, pl.ds(0, qc)]))
-        first.append(fetch(wc_ref.at[rows_in], win.at[me, h, :, pl.ds(qc + 2 * kc, cc)]))
+    first = [
+        fetch(wq_ref, win.at[me, :, :, pl.ds(0, qc)]),
+        fetch(wc_ref, win.at[me, :, :, pl.ds(qc + 2 * kc, cc)]),
+    ]
     own_tok = [fetch(tok_ref.at[:, pl.ds(b * depth, depth)], tok.at[t * per + b]) for b in range(per)]
     later = []
     for h in range(2):
@@ -271,28 +269,37 @@
         copy.wait()
     pl.semaphore_wait(barrier, len(peers))
 
-    def ring_copy(buf, send, recv, way, k, hop):
+    count = QUARTERS * (n - 1) // 2
+    last = count - 1
+
+    def ring_copy(buf, way, k, hop, turn):
         sign = -1 if way == 0 else 1
         q = k % QUARTERS if way == 0 else QUARTERS - 1 - k % QUARTERS
         o = at(pos + sign * (k // QUARTERS + hop))
         slot = buf.at[o, q] if buf is win else buf.at[o, q // 2, q % 2]
-        return rdma(slot, slot, send.at[way, k], recv.at[way, k], ring[way], t)
+        return rdma(slot, slot, ring_send.at[way, turn % SENDS], ring_recv.at[way, k], ring[way], t)
 
     def w_in(way, k, hop):
-        return ring_copy(win, win_send, win_recv, way, k, hop)
+        return ring_copy(win, way, k, hop, k)
 
     def w_out(way, k, hop):
-        return ring_copy(wout, wout_send, wout_recv, way, k, hop)
+        return ring_copy(wout, way, k, hop, count + k)
+
+    def launched(way, turn):
+        return w_in(way, turn, 0) if turn < count else w_out(way, turn - count, 0)
+
+    def launch(way, turn):
+        if turn >= SENDS:
+            launched(way, turn - SENDS).wait_send()
+        launched(way, turn).start()
 
     def tok_copy(owner, b, i, dst):
         slot = tok.at[owner * per + b]
         return rdma(slot, slot, tok_send.at[i], tok_recv.at[i], me, dst)
 
-    count = QUARTERS * (n - 1) // 2
-    last = count - 1
     for k in range(QUARTERS):
         for way in range(2):
-            w_in(way, k, 0).start()
+            launch(way, k)
     for copy in own_tok:
         copy.wait()
     for b in range(per):
@@ -320,16 +327,16 @@
         for way in range(2):
             copy(way, k, 1).wait_recv()
             if k + QUARTERS <= last:
-                copy(way, k + QUARTERS, 0).start()
+                launch(way, k + QUARTERS + (0 if copy is w_in else count))
 
     def start_out(k):
         for way in range(2):
-            w_out(way, k, 0).start()
+            launch(way, count + k)
 
     done_blocks = 0
     for k in range(count):
         relay(w_in, k)
-        if k in (last - 3, last - 2):
+        if last - 3 <= k < last:
             start_out(k - (last - 3))
         if k in (3, 6):
             b = 0 if k == 3 else 1
@@ -359,7 +366,6 @@
     rims = [rim(kv, WINDOW, True, 0), rim(kv, WINDOW, False, 1), rim(chan, RIM, True, 2), rim(chan, RIM, False, 3)]
     for c in rims:
         c.start()
-    start_out(2)
     start_out(3)
     query[...] = acc[:, 0:qc].astype(bf16)
 
@@ -423,14 +429,17 @@
         d, h = k // QUARTERS, (k % QUARTERS) // 2
         pieces += [(min(2 * d + 1, n - 1), h), (min(2 * d + 2, n - 1), 1 - h)]
 
-    def emit(i):
-        o, h = origin[pieces[i][0]], pieces[i][1]
-        got = jnp.dot(hidden[...], wout[o, h].reshape(qc + cc, half), preferred_element_type=f32)
-        part[o, h] = got.astype(bf16)
-
-        @pl.when(lax.rem(o // per, 2) != lax.rem(t, 2))
-        def _():
-            to_mate(o, h).start()
+    def emit(ids):
+        places = [(origin[pieces[i][0]], pieces[i][1]) for i in ids]
+        side = jnp.concatenate([wout[o, h].reshape(qc + cc, half) for o, h in places], axis=1)
+        got = jnp.dot(hidden[...], side, preferred_element_type=f32).astype(bf16)
+        for j, (o, h) in enumerate(places):
+            part[o, h] = got[:, j * half : (j + 1) * half]
+        for o, h in places:
+
+            @pl.when(lax.rem(o // per, 2) != lax.rem(t, 2))
+            def _(o=o, h=h):
+                to_mate(o, h).start()
 
     def combine(i):
         o, h = origin[pieces[i][0]], pieces[i][1]
@@ -448,30 +457,25 @@
 
     blocks = rows // WINDOW
     inner = list(range(1, blocks - 1))
-    emitted = combined = 0
+    emits = {6: range(0, 8), 7: range(8, 10), 9: range(10, 12), 11: range(12, 14), 13: range(14, 16)}
+    combines = {8: range(0, 8), 9: range(8, 10), 11: range(10, 12), 12: range(12, 14), 13: range(14, 16)}
     for k in range(count):
         relay(w_out, k)
         if k < 2:
             for b in inner[k :: 2]:
                 attend(b)
-        elif k == 2:
+        elif k == 3:
             for c in rims:
                 c.wait()
             attend(0)
-        elif k == 3:
+        elif k == 4:
             attend(blocks - 1)
-        elif k == 4:
+        elif k == 5:
             pool()
-        else:
-            here = 2 + 2 * ((k + 1) // 2)
-            goal = here if k == last else min(here, emitted + 3)
-            behind = emitted
-            while emitted < goal:
-                emit(emitted)
-                emitted += 1
-            while combined < (emitted if k == last else behind):
-                combine(combined)
-                combined += 1
+        if k in emits:
+            emit(emits[k])
+        for i in combines.get(k, ()):
+            combine(i)
 
     share = []
     for s in range(per):
@@ -498,10 +502,9 @@
             for h in range(2):
                 to_mate(o, h).wait_send()
 
-    for k in range(count):
+    for turn in range(2 * count - SENDS, 2 * count):
         for way in range(2):
-            w_in(way, k, 0).wait_send()
-            w_out(way, k, 0).wait_send()
+            launched(way, turn).wait_send()
     for b in range(per):
         tok_copy(t, b, b, across).wait_send()
         tok_copy(t, b, per + b, mate).wait_send()
@@ -557,9 +560,7 @@
             pltpu.VMEM(w_pool.shape, bf16),
             pltpu.VMEM((1, cc), f32),
             pltpu.VMEM((1, share), f32),
-            dma((2, count)),
-            dma((2, count)),
-            dma((2, count)),
+            dma((2, SENDS)),
             dma((2, count)),
             dma((3 * per,)),
             dma((3 * per,)),
@@ -568,7 +569,7 @@
             dma((n, 2)),
             dma((n, 2)),
             dma((per, 2)),
-            dma((2 * QUARTERS + per + 10,)),
+            dma((per + 12,)),
             dma((tp,)),
             dma((tp,)),
         ],
@@ -578,10 +579,10 @@
         name="mixer",
     )(
         pltpu.with_memory_space_constraint(tokens, pltpu.HBM),
-        pltpu.with_memory_space_constraint(w_query, pltpu.HBM),
+        pltpu.with_memory_space_constraint(w_query.reshape(QUARTERS, -1, qc), pltpu.HBM),
         pltpu.with_memory_space_constraint(w_key.T, pltpu.HBM),
         pltpu.with_memory_space_constraint(w_value.T, pltpu.HBM),
-        pltpu.with_memory_space_constraint(w_pool_in, pltpu.HBM),
+        pltpu.with_memory_space_constraint(w_pool_in.reshape(QUARTERS, -1, cc), pltpu.HBM),
         pltpu.with_memory_space_constraint(sink.reshape(1, -1), pltpu.HBM),
         pltpu.with_memory_space_constraint(w_pool, pltpu.HBM),
         pltpu.with_memory_space_constraint(pool_scale.reshape(1, -1), pltpu.HBM),

time: 66.3 us -> 64.9 us (0.979)
  Pallas kernels: 65.4 us -> 63.9 us
    pallas_call x1, Pallas kernels: 65.4 us -> 63.9 us  [fused(): pl.pallas_call(functools.partial(mixer_kernel, n, tp), out_shape=jax.Shap...]
where the time goes in v2:
time: 64.9 us; the launch traced here: 64.7 us
  Pallas kernels  63.9 us (98%)
  local copies, waits for them, and re-layouts  0.8 us (1%)
    pallas_call x1, Pallas kernels, fused(): pl.pallas_call(functools.partial(mixer_kernel, n, tp), out_shape=jax.Shap...  63.9 us

profile of v2, /device:TPU:0, one launch (start us, length us, event | category | flops | bytes accessed | tf_op | source)
XLA Modules:
  0.0 64.7 jit_solution(12611710069467785690)
XLA Ops:
  0.0 63.9 %mixer.1 = bf16[512,512]{1,0:T(8,128)(2,1)S(1)} custom-call(bf16[512,512]{1,0:T(8,128)(2,1)} %tok_ref.1, bf16[4,64,256]{2,1,0:T(8,128)(2,1)} %bitcast.7, bf16[64,256]{1,0:T(8,128)(2,1)} %bitcast.9, bf16[64,256]{1,0:T(8,128)(2,1)} %bitcast.10, bf16[4,64,256]{2,1,0:T(8,128)(2,1)} %bitcast.8, f32[1,4]{1,0:T(1,128)} %bitcast.13, bf16[1,256,256]{2,1,0:T(8,128)(2,1)} %wp_ref.1, ...), custom_call_target="tpu_custom_call" | custom-call | tf_op jit(solution)/shard_map/mixer/pallas_call | solution.py:539
  63.9 0.8 %copy.13 = bf16[512,512]{1,0:T(8,128)(2,1)} copy(bf16[512,512]{1,0:T(8,128)(2,1)S(1)} %mixer.1) | data formatting | bytes 1048576

commit v3 on v2

--- a/solution.py
+++ b/solution.py
@@ -179,6 +179,9 @@
     landed,
     own,
     stats,
+    late,
+    echo,
+    sums,
     pair_in,
     sinks,
     wpool,
@@ -190,12 +193,17 @@
     tok_recv,
     rim_send,
     rim_recv,
+    mate_send,
+    mate_recv,
     part_send,
-    mate_recv,
     part_recv,
+    echo_send,
+    echo_recv,
     load,
     stat_send,
     stat_recv,
+    late_send,
+    late_recv,
 ):
     f32, bf16 = jnp.float32, jnp.bfloat16
     me, t = lax.axis_index("sp"), lax.axis_index("tp")
@@ -306,6 +314,7 @@
         tok_copy(t, b, b, across).start()
     for b in range(per):
         tok_copy(t, b, per + b, mate).start()
+
     for copy in later:
         copy.wait()
 
@@ -394,113 +403,229 @@
             outs.append((raised * (1.0 / total)).astype(bf16))
         got = jnp.dot(jnp.concatenate(outs, axis=0), band, preferred_element_type=f32)
         got = got[:, HEAD_DIM : 2 * HEAD_DIM].astype(bf16)
-        hidden[b * WINDOW : (b + 1) * WINDOW, 0:qc] = jnp.concatenate(
+        hidden[place(b) : place(b) + WINDOW, 0:qc] = jnp.concatenate(
             [got[g * WINDOW : (g + 1) * WINDOW] for g in range(group)], axis=1
         )
 
-    def pool():
-        length = rows + 2 * RIM
-        e = chan[...].astype(f32)
-        p = lax.broadcasted_iota(jnp.int32, (length, 1), 0) + (me * rows - RIM)
+    blocks = rows // WINDOW
+    order = list(range(1, blocks - 1)) + [0, blocks - 1]
+    early = (blocks - 2) * WINDOW
+
+    def place(b):
+        return order.index(b) * WINDOW
+
+    half_width = 1
+    for level in range(1, POOL_GROUPS):
+        half_width = jnp.where(t == level, 2**level, half_width)
+
+    def spread_of(start, size):
+        length = size + 2 * RIM
+        e = chan[start : start + length].astype(f32)
+        p = lax.broadcasted_iota(jnp.int32, (length, 1), 0) + (me * rows + start - RIM)
         e = jnp.where((p >= 0) & (p < seq_len), e, 0.0)
-        sums = e + pltpu.roll(e, 1, 0)
-        pick = sums
+        total = e + pltpu.roll(e, 1, 0)
+        pick = total
         for level in range(1, POOL_GROUPS):
             step = 2 ** (level - 1)
-            sums = pltpu.roll(sums, step, 0) + pltpu.roll(sums, length - step, 0)
-            pick = jnp.where(t == level, sums, pick)
-        half_width = 1
-        for level in range(1, POOL_GROUPS):
-            half_width = jnp.where(t == level, 2**level, half_width)
+            total = pltpu.roll(total, step, 0) + pltpu.roll(total, length - step, 0)
+            pick = jnp.where(t == level, total, pick)
         number = (jnp.clip(p + half_width, 0, seq_len) - jnp.clip(p - half_width, 0, seq_len)).astype(f32)
-        spread = (pick[RIM : RIM + rows] / number[RIM : RIM + rows] - e[RIM : RIM + rows]).astype(bf16)
-        got = jnp.dot(spread, wpool[0], preferred_element_type=f32)
-        hidden[:, qc:] = (got * scales[...]).astype(bf16)
-
-    def to_mate(o, h):
-        return rdma(part.at[o, h], mated.at[o, h], part_send.at[o, h], mate_recv.at[o, h], me, mate)
-
-    def to_owner(o, h):
-        s = lax.rem(o, per)
-        return rdma(part.at[o, h], landed.at[s, h], part_send.at[o, h], part_recv.at[s, h], me, across)
+        return (pick[RIM : RIM + size] / number[RIM : RIM + size] - e[RIM : RIM + size]).astype(bf16)
+
+    def pooled_of(spread):
+        return (jnp.dot(spread, wpool[0], preferred_element_type=f32) * scales[...]).astype(bf16)
+
+    def pool_inner():
+        got = pooled_of(spread_of(RIM, rows - 2 * RIM))
+        for b in range(blocks):
+            low, high = max(b * WINDOW, RIM), min((b + 1) * WINDOW, rows - RIM)
+            base = place(b) - b * WINDOW
+            hidden[base + low : base + high, qc:] = got[low - RIM : high - RIM]
+
+    def pool_edges():
+        got = pooled_of(jnp.concatenate([spread_of(0, RIM), spread_of(rows - RIM, RIM)], axis=0))
+        hidden[place(0) : place(0) + RIM, qc:] = got[0:RIM]
+        end = place(blocks - 1) + WINDOW
+        hidden[end - RIM : end, qc:] = got[RIM:]
+
+    near = 3
+    spans = (pl.ds(0, early), pl.ds(early, rows - early))
+
+    def unit(buf, o, u, split):
+        return buf.at[o, :, spans[u]] if split else buf.at[o, u]
+
+    def to_mate(o, u, split):
+        i = (o // (2 * per)) * per + lax.rem(o, per)
+        return rdma(
+            unit(part, o, u, split), unit(mated, o, u, split), mate_send.at[i, u], mate_recv.at[i, u], me, mate
+        )
+
+    def to_owner(o, u, split):
+        i = lax.rem(o, per)
+        return rdma(
+            unit(part, o, u, split), unit(landed, i, u, split), part_send.at[i, u], part_recv.at[i, u], me, across
+        )
+
+    final = origin[n - 1]
+    holder = final // per
+
+    def to_echo(h):
+        return rdma(part.at[final, h], echo.at[h], echo_send.at[h], echo_recv.at[h], me, across)
+
+    def to_late():
+        return rdma(late, late, late_send.at[0], late_recv.at[0], me, mate)
 
     pieces = [(0, 0), (0, 1)]
     for k in range(1, count, 2):
         d, h = k // QUARTERS, (k % QUARTERS) // 2
         pieces += [(min(2 * d + 1, n - 1), h), (min(2 * d + 2, n - 1), 1 - h)]
 
-    def emit(ids):
-        places = [(origin[pieces[i][0]], pieces[i][1]) for i in ids]
-        side = jnp.concatenate([wout[o, h].reshape(qc + cc, half) for o, h in places], axis=1)
-        got = jnp.dot(hidden[...], side, preferred_element_type=f32).astype(bf16)
-        for j, (o, h) in enumerate(places):
-            part[o, h] = got[:, j * half : (j + 1) * half]
-        for o, h in places:
+    def emit(places, span, split):
+        side = jnp.concatenate([wout[origin[i], h].reshape(qc + cc, half) for i, h in places], axis=1)
+        got = jnp.dot(hidden[span, :], side, preferred_element_type=f32).astype(bf16)
+        for j, (i, h) in enumerate(places):
+            part[origin[i], h, span] = got[:, j * half : (j + 1) * half]
+        sent = [(i, spans.index(span)) for i, h in places if h == 0] if split else places
+        for i, u in sent:
+            o = origin[i]
 
             @pl.when(lax.rem(o // per, 2) != lax.rem(t, 2))
-            def _(o=o, h=h):
-                to_mate(o, h).start()
-
-    def combine(i):
-        o, h = origin[pieces[i][0]], pieces[i][1]
+            def _(o=o, u=u):
+                to_mate(o, u, split).start()
+
+    def emit_near(u):
+        emit([(i, h) for i in range(near) for h in range(2)], spans[u], True)
+
+    def emit_far(ids):
+        emit([pieces[i] for i in ids], pl.ds(0, rows), False)
+
+    def combine(i, u, split):
+        o = origin[i]
+        where = (slice(None), spans[u]) if split else (u,)
 
         @pl.when(o // per == t)
         def _():
-            to_mate(o, h).wait_recv()
-            own[lax.rem(o, per), h] = part[o, h].astype(f32) + mated[o, h].astype(f32)
+            to_mate(o, u, split).wait_recv()
+            both = part[(o,) + where].astype(f32) + mated[(o,) + where].astype(f32)
+            own[(lax.rem(o, per),) + where] = both
+            if i == n - 1:
+                part[(o,) + where] = both.astype(bf16)
+                to_echo(u).start()
 
         @pl.when(o // per == across)
         def _():
-            to_mate(o, h).wait_recv()
-            part[o, h] = (part[o, h].astype(f32) + mated[o, h].astype(f32)).astype(bf16)
-            to_owner(o, h).start()
-
-    blocks = rows // WINDOW
-    inner = list(range(1, blocks - 1))
-    emits = {6: range(0, 8), 7: range(8, 10), 9: range(10, 12), 11: range(12, 14), 13: range(14, 16)}
-    combines = {8: range(0, 8), 9: range(8, 10), 11: range(10, 12), 12: range(12, 14), 13: range(14, 16)}
+            to_mate(o, u, split).wait_recv()
+            both = part[(o,) + where].astype(f32) + mated[(o,) + where].astype(f32)
+            part[(o,) + where] = both.astype(bf16)
+            to_owner(o, u, split).start()
+
+    def combine_near(u):
+        for i in range(near):
+            combine(i, u, True)
+
+    def combine_far(ids):
+        for i in ids:
+            combine(pieces[i][0], pieces[i][1], False)
+
+    def pack(one, two):
+        one = jnp.sum(one, axis=1, keepdims=True)
+        two = jnp.sum(two, axis=1, keepdims=True)
+        lane = lax.broadcasted_iota(jnp.int32, (rows, 128), 1)
+        return jnp.transpose(jnp.where(lane == 0, one, jnp.where(lane == 1, two, 0.0)))[0:8]
+
+    sums[...] = jnp.zeros_like(sums)
+    emits = {5: (6, 8), 7: (8, 10), 9: (10, 12), 11: (12, 14), 13: (14, 16)}
+    combines = {7: (6, 8), 8: (8, 10), 10: (10, 12), 12: (12, 14), 13: (14, 16)}
     for k in range(count):
         relay(w_out, k)
         if k < 2:
-            for b in inner[k :: 2]:
+            for b in order[: blocks - 2][k::2]:
                 attend(b)
+        elif k == 2:
+            pool_inner()
         elif k == 3:
+            emit_near(0)
             for c in rims:
                 c.wait()
             attend(0)
         elif k == 4:
             attend(blocks - 1)
-        elif k == 5:
-            pool()
+            combine_near(0)
+            pool_edges()
+            emit_near(1)
+        elif k == 6:
+            combine_near(1)
         if k in emits:
-            emit(emits[k])
-        for i in combines.get(k, ()):
-            combine(i)
-
-    share = []
-    for s in range(per):
-        for h in range(2):
-            to_owner(t * per + s, h).wait_recv()
-            share.append(own[s, h] + landed[s, h].astype(f32))
-    mix = jnp.concatenate(share, axis=1)
-    acc[:, 0 : mix.shape[1]] = mix
-    one = jnp.sum(mix, axis=1, keepdims=True)
-    two = jnp.sum(mix * mix, axis=1, keepdims=True)
-    lane = lax.broadcasted_iota(jnp.int32, (rows, 128), 1)
-    both = jnp.where(lane == 0, one, jnp.where(lane == 1, two, 0.0))
-    stats[t] = jnp.transpose(both)[0:8]
+            emit_far(range(*emits[k]))
+        combine_far(range(*combines.get(k, (0, 0))))
 
     def stat_copy(j):
         return rdma(stats.at[t], stats.at[t], stat_send.at[j], stat_recv.at[t], me, lax.rem(t + j, tp))
 
+    for i in range(n - 1):
+        o = origin[i]
+
+        @pl.when(o // per == t)
+        def _(o=o, i=i):
+            for u in range(2):
+                to_owner(o, u, i < near).wait_recv()
+
+    for i in range(per):
+        o = t * per + i
+
+        @pl.when(o != final)
+        def _(o=o, i=i):
+            one = two = 0.0
+            for h in range(2):
+                mix = own[i, h] + landed[i, h].astype(f32)
+                acc[:, (2 * i + h) * half : (2 * i + h + 1) * half] = mix
+                one, two = one + mix, two + mix * mix
+            sums[0] += one
+            sums[1] += two
+
+    stats[t] = pack(sums[0], sums[1])
     for j in range(1, tp):
         stat_copy(j).start()
-    for o in range(n):
-
-        @pl.when(o // per != t)
-        def _():
-            for h in range(2):
-                to_mate(o, h).wait_send()
+
+    @pl.when(holder == t)
+    def _():
+        one = two = 0.0
+        for h in range(2):
+            i = lax.rem(final, per)
+            to_owner(final, h, False).wait_recv()
+            mix = own[i, h] + landed[i, h].astype(f32)
+            acc[:, pl.ds(pl.multiple_of((2 * i + h) * half, 128), half)] = mix
+            one, two = one + mix, two + mix * mix
+        late[...] = pack(one, two)
+        to_late().start()
+
+    @pl.when(holder == across)
+    def _():
+        one = two = 0.0
+        for h in range(2):
+            to_echo(h).wait_recv()
+            mix = part[final, h].astype(f32) + echo[h].astype(f32)
+            one, two = one + mix, two + mix * mix
+        late[...] = pack(one, two)
+        to_late().start()
+
+    for i in range(n):
+        o = origin[i]
+
+        @pl.when(lax.rem(o // per, 2) != lax.rem(t, 2))
+        def _(o=o, i=i):
+            for u in range(2):
+                to_mate(o, u, i < near).wait_send()
+
+        @pl.when(o // per == across)
+        def _(o=o, i=i):
+            for u in range(2):
+                to_owner(o, u, i < near).wait_send()
+
+    @pl.when(holder == t)
+    def _():
+        for h in range(2):
+            to_echo(h).wait_send()
 
     for turn in range(2 * count - SENDS, 2 * count):
         for way in range(2):
@@ -512,7 +637,13 @@
     for j in range(1, tp):
         src = lax.rem(t + j, tp)
         rdma(stats.at[src], stats.at[src], stat_send.at[j], stat_recv.at[src], me, src).wait_recv()
-    totals = stats[0]
+    paired = lax.rem(holder, 2) == lax.rem(t, 2)
+
+    @pl.when(jnp.logical_not(paired))
+    def _():
+        to_late().wait_recv()
+
+    totals = late[...] + stats[0]
     for i in range(1, tp):
         totals = totals + stats[i]
     tall = jnp.concatenate([totals, jnp.zeros((120, rows), f32)], axis=0)
@@ -521,9 +652,15 @@
     row_mean = back[:, 0:1] / width
     variance = back[:, 1:2] / width - row_mean * row_mean
     scale = lax.rsqrt(variance + epsilon)
-    out_ref[...] = ((acc[:, 0 : gain_ref.shape[1]] - row_mean) * scale * gains[...]).astype(bf16)
+    normed = ((acc[:, 0 : gain_ref.shape[1]] - row_mean) * scale * gains[...]).astype(bf16)
+    for b in range(blocks):
+        out_ref[b * WINDOW : (b + 1) * WINDOW, :] = normed[place(b) : place(b) + WINDOW]
     for j in range(1, tp):
         stat_copy(j).wait_send()
+
+    @pl.when(paired)
+    def _():
+        to_late().wait_send()
 
 
 def fused(n, tp, tokens, w_query, w_key, w_value, w_pool_in, sink, w_pool, pool_scale, w_out_attn, w_out_pool, out_gain):
@@ -555,6 +692,9 @@
             pltpu.VMEM((per, 2, rows, half), bf16),
             pltpu.VMEM((per, 2, rows, half), f32),
             pltpu.VMEM((tp, 8, rows), f32),
+            pltpu.VMEM((8, rows), f32),
+            pltpu.VMEM((2, rows, half), bf16),
+            pltpu.VMEM((2, rows, half), f32),
             pltpu.VMEM((2 * kc, depth), bf16),
             pltpu.VMEM((1, sink.shape[0]), f32),
             pltpu.VMEM(w_pool.shape, bf16),
@@ -566,12 +706,17 @@
             dma((3 * per,)),
             dma((4,)),
             dma((4,)),
-            dma((n, 2)),
-            dma((n, 2)),
+            dma((n // 2, 2)),
+            dma((n // 2, 2)),
             dma((per, 2)),
+            dma((per, 2)),
+            dma((2,)),
+            dma((2,)),
             dma((per + 12,)),
             dma((tp,)),
             dma((tp,)),
+            dma((1,)),
+            dma((1,)),
         ],
         compiler_params=pltpu.CompilerParams(
             collective_id=0, has_side_effects=True, vmem_limit_bytes=32 * 1024 * 1024
@@ -602,7 +747,7 @@
         and w_pool.shape[0] == 1
         and w_out_attn.shape[1] % 256 == 0
         and w_out_attn.shape[0] == w_query.shape[1]
-        and tokens.shape[0] >= 2 * WINDOW
+        and tokens.shape[0] >= 3 * WINDOW
     )
 
 

time: 64.9 us -> 62.8 us (0.968)
  Pallas kernels: 63.9 us -> 61.9 us
    pallas_call x1, Pallas kernels: 63.9 us -> 61.9 us  [fused(): pl.pallas_call(functools.partial(mixer_kernel, n, tp), out_shape=jax.Shap...]
where the time goes in v3:
time: 62.8 us; the launch traced here: 62.7 us
  Pallas kernels  61.9 us (99%)
  local copies, waits for them, and re-layouts  0.8 us (1%)
    pallas_call x1, Pallas kernels, fused(): pl.pallas_call(functools.partial(mixer_kernel, n, tp), out_shape=jax.Shap...  61.9 us

profile of v3, /device:TPU:0, one launch (start us, length us, event | category | flops | bytes accessed | tf_op | source)
XLA Modules:
  0.0 62.7 jit_solution(10894858428800289338)
XLA Ops:
  0.0 61.9 %mixer.1 = bf16[512,512]{1,0:T(8,128)(2,1)S(1)} custom-call(bf16[512,512]{1,0:T(8,128)(2,1)} %tok_ref.1, bf16[4,64,256]{2,1,0:T(8,128)(2,1)} %bitcast.7, bf16[64,256]{1,0:T(8,128)(2,1)} %bitcast.9, bf16[64,256]{1,0:T(8,128)(2,1)} %bitcast.10, bf16[4,64,256]{2,1,0:T(8,128)(2,1)} %bitcast.8, f32[1,4]{1,0:T(1,128)} %bitcast.13, bf16[1,256,256]{2,1,0:T(8,128)(2,1)} %wp_ref.1, ...), custom_call_target="tpu_custom_call" | custom-call | tf_op jit(solution)/shard_map/mixer/pallas_call | solution.py:676
  61.9 0.8 %copy.13 = bf16[512,512]{1,0:T(8,128)(2,1)} copy(bf16[512,512]{1,0:T(8,128)(2,1)S(1)} %mixer.1) | data formatting | bytes 1048576

commit v4 on v3

--- a/solution.py
+++ b/solution.py
@@ -148,7 +148,8 @@
 MESH = pl.DeviceIdType.MESH
 RIM = 16
 QUARTERS = 4
-SENDS = 8
+SENDS = 6
+RECVS = 10
 
 
 def mixer_kernel(
@@ -241,8 +242,8 @@
     wide = woa_ref.shape[1]
     half = wide // 2
     barrier = pltpu.get_barrier_semaphore()
-    peers = [(s, t) for s in ring] + [(s, t) for s in (before, after)]
-    peers += [(me, lax.rem(t + i, tp)) for i in range(1, tp)]
+    peers = [(s, t) for s in ring]
+    peers += [(me, mate), (me, across)]
     for s, p in peers:
         pl.semaphore_signal(barrier, inc=1, device_id={"sp": s, "tp": p}, device_id_type=MESH)
 
@@ -285,7 +286,7 @@
         q = k % QUARTERS if way == 0 else QUARTERS - 1 - k % QUARTERS
         o = at(pos + sign * (k // QUARTERS + hop))
         slot = buf.at[o, q] if buf is win else buf.at[o, q // 2, q % 2]
-        return rdma(slot, slot, ring_send.at[way, turn % SENDS], ring_recv.at[way, k], ring[way], t)
+        return rdma(slot, slot, ring_send.at[way, turn % SENDS], ring_recv.at[way, turn % RECVS], ring[way], t)
 
     def w_in(way, k, hop):
         return ring_copy(win, way, k, hop, k)
@@ -701,7 +702,7 @@
             pltpu.VMEM((1, cc), f32),
             pltpu.VMEM((1, share), f32),
             dma((2, SENDS)),
-            dma((2, count)),
+            dma((2, RECVS)),
             dma((3 * per,)),
             dma((3 * per,)),
             dma((4,)),

time: 62.8 us -> 61.3 us (0.976)
  Pallas kernels: 61.9 us -> 60.3 us
    pallas_call x1, Pallas kernels: 61.9 us -> 60.3 us  [fused(): pl.pallas_call(functools.partial(mixer_kernel, n, tp), out_shape=jax.Shap...]
where the time goes in v4:
time: 61.3 us; the launch traced here: 61.1 us
  Pallas kernels  60.3 us (98%)
  local copies, waits for them, and re-layouts  0.8 us (1%)
    pallas_call x1, Pallas kernels, fused(): pl.pallas_call(functools.partial(mixer_kernel, n, tp), out_shape=jax.Shap...  60.3 us

profile of v4, /device:TPU:0, one launch (start us, length us, event | category | flops | bytes accessed | tf_op | source)
XLA Modules:
  0.0 61.1 jit_solution(5929137706856635733)
XLA Ops:
  0.0 60.3 %mixer.1 = bf16[512,512]{1,0:T(8,128)(2,1)S(1)} custom-call(bf16[512,512]{1,0:T(8,128)(2,1)} %tok_ref.1, bf16[4,64,256]{2,1,0:T(8,128)(2,1)} %bitcast.7, bf16[64,256]{1,0:T(8,128)(2,1)} %bitcast.9, bf16[64,256]{1,0:T(8,128)(2,1)} %bitcast.10, bf16[4,64,256]{2,1,0:T(8,128)(2,1)} %bitcast.8, f32[1,4]{1,0:T(1,128)} %bitcast.13, bf16[1,256,256]{2,1,0:T(8,128)(2,1)} %wp_ref.1, ...), custom_call_target="tpu_custom_call" | custom-call | tf_op jit(solution)/shard_map/mixer/pallas_call | solution.py:677
  60.4 0.8 %copy.13 = bf16[512,512]{1,0:T(8,128)(2,1)} copy(bf16[512,512]{1,0:T(8,128)(2,1)S(1)} %mixer.1) | data formatting | bytes 1048576

commit v5 on v4

--- a/solution.py
+++ b/solution.py
@@ -304,7 +304,7 @@
 
     def tok_copy(owner, b, i, dst):
         slot = tok.at[owner * per + b]
-        return rdma(slot, slot, tok_send.at[i], tok_recv.at[i], me, dst)
+        return rdma(slot, slot, tok_send.at[0], tok_recv.at[i], me, dst)
 
     for k in range(QUARTERS):
         for way in range(2):
@@ -458,20 +458,20 @@
     def to_mate(o, u, split):
         i = (o // (2 * per)) * per + lax.rem(o, per)
         return rdma(
-            unit(part, o, u, split), unit(mated, o, u, split), mate_send.at[i, u], mate_recv.at[i, u], me, mate
+            unit(part, o, u, split), unit(mated, o, u, split), mate_send.at[0], mate_recv.at[i, u], me, mate
         )
 
     def to_owner(o, u, split):
         i = lax.rem(o, per)
         return rdma(
-            unit(part, o, u, split), unit(landed, i, u, split), part_send.at[i, u], part_recv.at[i, u], me, across
+            unit(part, o, u, split), unit(landed, i, u, split), part_send.at[0], part_recv.at[i, u], me, across
         )
 
     final = origin[n - 1]
     holder = final // per
 
     def to_echo(h):
-        return rdma(part.at[final, h], echo.at[h], echo_send.at[h], echo_recv.at[h], me, across)
+        return rdma(part.at[final, h], echo.at[h], echo_send.at[0], echo_recv.at[h], me, across)
 
     def to_late():
         return rdma(late, late, late_send.at[0], late_recv.at[0], me, mate)
@@ -536,7 +536,15 @@
 
     sums[...] = jnp.zeros_like(sums)
     emits = {5: (6, 8), 7: (8, 10), 9: (10, 12), 11: (12, 14), 13: (14, 16)}
-    combines = {7: (6, 8), 8: (8, 10), 10: (10, 12), 12: (12, 14), 13: (14, 16)}
+    odd = lax.rem(t, 2) == 1
+    ahead = {6: (6, 8), 7: (8, 10), 9: (10, 12), 11: (12, 14)}
+    behind = {7: (6, 8), 8: (8, 10), 10: (10, 12), 13: (12, 14)}
+
+    def on(core, work, *args):
+        @pl.when(odd == core)
+        def _():
+            work(*args)
+
     for k in range(count):
         relay(w_out, k)
         if k < 2:
@@ -549,19 +557,26 @@
             for c in rims:
                 c.wait()
             attend(0)
+            on(False, combine_near, 0)
         elif k == 4:
             attend(blocks - 1)
-            combine_near(0)
+            on(True, combine_near, 0)
             pool_edges()
             emit_near(1)
-        elif k == 6:
-            combine_near(1)
         if k in emits:
             emit_far(range(*emits[k]))
-        combine_far(range(*combines.get(k, (0, 0))))
+        if k == 5:
+            on(False, combine_near, 1)
+        elif k == 6:
+            on(True, combine_near, 1)
+        if k in ahead:
+            on(False, combine_far, range(*ahead[k]))
+        if k in behind:
+            on(True, combine_far, range(*behind[k]))
+    combine_far(range(14, 16))
 
     def stat_copy(j):
-        return rdma(stats.at[t], stats.at[t], stat_send.at[j], stat_recv.at[t], me, lax.rem(t + j, tp))
+        return rdma(stats.at[t], stats.at[t], stat_send.at[0], stat_recv.at[t], me, lax.rem(t + j, tp))
 
     for i in range(n - 1):
         o = origin[i]
@@ -610,34 +625,24 @@
         late[...] = pack(one, two)
         to_late().start()
 
-    for i in range(n):
-        o = origin[i]
-
-        @pl.when(lax.rem(o // per, 2) != lax.rem(t, 2))
-        def _(o=o, i=i):
-            for u in range(2):
-                to_mate(o, u, i < near).wait_send()
-
-        @pl.when(o // per == across)
-        def _(o=o, i=i):
-            for u in range(2):
-                to_owner(o, u, i < near).wait_send()
+    def drain(buf, amount, sem):
+        whole = buf.at[pl.ds(0, amount)]
+        rdma(whole, whole, sem.at[0], mate_recv.at[0, 0], me, mate).wait_send()
+
+    drain(part, n // 2, mate_send)
+    drain(part, per, part_send)
+    drain(tok, 3 * per, tok_send)
 
     @pl.when(holder == t)
     def _():
-        for h in range(2):
-            to_echo(h).wait_send()
+        drain(part, 1, echo_send)
 
     for turn in range(2 * count - SENDS, 2 * count):
         for way in range(2):
             launched(way, turn).wait_send()
-    for b in range(per):
-        tok_copy(t, b, b, across).wait_send()
-        tok_copy(t, b, per + b, mate).wait_send()
-        tok_copy(across, b, 2 * per + b, mate).wait_send()
     for j in range(1, tp):
         src = lax.rem(t + j, tp)
-        rdma(stats.at[src], stats.at[src], stat_send.at[j], stat_recv.at[src], me, src).wait_recv()
+        rdma(stats.at[src], stats.at[src], stat_send.at[0], stat_recv.at[src], me, src).wait_recv()
     paired = lax.rem(holder, 2) == lax.rem(t, 2)
 
     @pl.when(jnp.logical_not(paired))
@@ -656,8 +661,7 @@
     normed = ((acc[:, 0 : gain_ref.shape[1]] - row_mean) * scale * gains[...]).astype(bf16)
     for b in range(blocks):
         out_ref[b * WINDOW : (b + 1) * WINDOW, :] = normed[place(b) : place(b) + WINDOW]
-    for j in range(1, tp):
-        stat_copy(j).wait_send()
+    drain(stats, tp - 1, stat_send)
 
     @pl.when(paired)
     def _():
@@ -703,18 +707,18 @@
             pltpu.VMEM((1, share), f32),
             dma((2, SENDS)),
             dma((2, RECVS)),
-            dma((3 * per,)),
+            dma((1,)),
             dma((3 * per,)),
             dma((4,)),
             dma((4,)),
+            dma((1,)),
             dma((n // 2, 2)),
-            dma((n // 2, 2)),
+            dma((1,)),
             dma((per, 2)),
-            dma((per, 2)),
-            dma((2,)),
+            dma((1,)),
             dma((2,)),
             dma((per + 12,)),
-            dma((tp,)),
+            dma((1,)),
             dma((tp,)),
             dma((1,)),
             dma((1,)),

time: 61.3 us -> 61.2 us (level)
  no operation moved by 1% of the time
where the time goes in v5:
time: 61.2 us; the launch traced here: 61 us
  Pallas kernels  60.2 us (98%)
  local copies, waits for them, and re-layouts  0.8 us (1%)
    pallas_call x1, Pallas kernels, fused(): pl.pallas_call(functools.partial(mixer_kernel, n, tp), out_shape=jax.Shap...  60.2 us

profile of v5, /device:TPU:0, one launch (start us, length us, event | category | flops | bytes accessed | tf_op | source)
XLA Modules:
  0.0 61.0 jit_solution(656637524796633446)
XLA Ops:
  0.0 60.2 %mixer.1 = bf16[512,512]{1,0:T(8,128)(2,1)S(1)} custom-call(bf16[512,512]{1,0:T(8,128)(2,1)} %tok_ref.1, bf16[4,64,256]{2,1,0:T(8,128)(2,1)} %bitcast.7, bf16[64,256]{1,0:T(8,128)(2,1)} %bitcast.9, bf16[64,256]{1,0:T(8,128)(2,1)} %bitcast.10, bf16[4,64,256]{2,1,0:T(8,128)(2,1)} %bitcast.8, f32[1,4]{1,0:T(1,128)} %bitcast.13, bf16[1,256,256]{2,1,0:T(8,128)(2,1)} %wp_ref.1, ...), custom_call_target="tpu_custom_call" | custom-call | tf_op jit(solution)/shard_map/mixer/pallas_call | solution.py:681
  60.3 0.8 %copy.13 = bf16[512,512]{1,0:T(8,128)(2,1)} copy(bf16[512,512]{1,0:T(8,128)(2,1)S(1)} %mixer.1) | data formatting | bytes 1048576

commit v6 on v5

--- a/solution.py
+++ b/solution.py
@@ -283,9 +283,14 @@
 
     def ring_copy(buf, way, k, hop, turn):
         sign = -1 if way == 0 else 1
-        q = k % QUARTERS if way == 0 else QUARTERS - 1 - k % QUARTERS
+        q = k % QUARTERS
         o = at(pos + sign * (k // QUARTERS + hop))
-        slot = buf.at[o, q] if buf is win else buf.at[o, q // 2, q % 2]
+        if buf is win:
+            slot = buf.at[o, q if way == 0 else QUARTERS - 1 - q]
+        elif k >= last - 1:
+            slot = buf.at[o, q, way]
+        else:
+            slot = buf.at[o, q // 2, (q + way) % 2]
         return rdma(slot, slot, ring_send.at[way, turn % SENDS], ring_recv.at[way, turn % RECVS], ring[way], t)
 
     def w_in(way, k, hop):
@@ -336,8 +341,13 @@
     def relay(copy, k):
         for way in range(2):
             copy(way, k, 1).wait_recv()
-            if k + QUARTERS <= last:
-                launch(way, k + QUARTERS + (0 if copy is w_in else count))
+            if copy is w_in:
+                if k + QUARTERS <= last:
+                    launch(way, k + QUARTERS)
+            elif k + QUARTERS < last:
+                launch(way, count + k + QUARTERS)
+            elif k == last - 3:
+                launch(way, count + last)
 
     def start_out(k):
         for way in range(2):
@@ -477,9 +487,10 @@
         return rdma(late, late, late_send.at[0], late_recv.at[0], me, mate)
 
     pieces = [(0, 0), (0, 1)]
-    for k in range(1, count, 2):
+    for k in range(1, count - 2, 2):
         d, h = k // QUARTERS, (k % QUARTERS) // 2
-        pieces += [(min(2 * d + 1, n - 1), h), (min(2 * d + 2, n - 1), 1 - h)]
+        pieces += [(2 * d + 1, h), (2 * d + 2, h)]
+    pieces += [(n - 1, 0), (n - 1, 1)]
 
     def emit(places, span, split):
         side = jnp.concatenate([wout[origin[i], h].reshape(qc + cc, half) for i, h in places], axis=1)
@@ -535,10 +546,10 @@
         return jnp.transpose(jnp.where(lane == 0, one, jnp.where(lane == 1, two, 0.0)))[0:8]
 
     sums[...] = jnp.zeros_like(sums)
-    emits = {5: (6, 8), 7: (8, 10), 9: (10, 12), 11: (12, 14), 13: (14, 16)}
+    emits = {5: (6, 8), 7: (8, 10), 9: (10, 12), 11: (12, 14), 12: (14, 15), 13: (15, 16)}
     odd = lax.rem(t, 2) == 1
-    ahead = {6: (6, 8), 7: (8, 10), 9: (10, 12), 11: (12, 14)}
-    behind = {7: (6, 8), 8: (8, 10), 10: (10, 12), 13: (12, 14)}
+    ahead = {6: (6, 8), 7: (8, 10), 9: (10, 12), 11: (12, 14), 12: (14, 15), 13: (15, 16)}
+    behind = {7: (6, 8), 8: (8, 10), 10: (10, 12), 13: (12, 16)}
 
     def on(core, work, *args):
         @pl.when(odd == core)
@@ -573,7 +584,6 @@
             on(False, combine_far, range(*ahead[k]))
         if k in behind:
             on(True, combine_far, range(*behind[k]))
-    combine_far(range(14, 16))
 
     def stat_copy(j):
         return rdma(stats.at[t], stats.at[t], stat_send.at[0], stat_recv.at[t], me, lax.rem(t + j, tp))

time: 61.2 us -> 60.5 us (0.989)
  Pallas kernels: 60.2 us -> 59.2 us
    pallas_call x1, Pallas kernels: 60.2 us -> 59.2 us  [fused(): pl.pallas_call(functools.partial(mixer_kernel, n, tp), out_shape=jax.Shap...]
where the time goes in v6:
time: 60.5 us; the launch traced here: 60 us
  Pallas kernels  59.2 us (98%)
  local copies, waits for them, and re-layouts  0.8 us (1%)
    pallas_call x1, Pallas kernels, fused(): pl.pallas_call(functools.partial(mixer_kernel, n, tp), out_shape=jax.Shap...  59.2 us

profile of v6, /device:TPU:0, one launch (start us, length us, event | category | flops | bytes accessed | tf_op | source)
XLA Modules:
  0.0 60.0 jit_solution(10065783383482022914)
XLA Ops:
  0.0 59.2 %mixer.1 = bf16[512,512]{1,0:T(8,128)(2,1)S(1)} custom-call(bf16[512,512]{1,0:T(8,128)(2,1)} %tok_ref.1, bf16[4,64,256]{2,1,0:T(8,128)(2,1)} %bitcast.7, bf16[64,256]{1,0:T(8,128)(2,1)} %bitcast.9, bf16[64,256]{1,0:T(8,128)(2,1)} %bitcast.10, bf16[4,64,256]{2,1,0:T(8,128)(2,1)} %bitcast.8, f32[1,4]{1,0:T(1,128)} %bitcast.13, bf16[1,256,256]{2,1,0:T(8,128)(2,1)} %wp_ref.1, ...), custom_call_target="tpu_custom_call" | custom-call | tf_op jit(solution)/shard_map/mixer/pallas_call | solution.py:691
  59.2 0.8 %copy.13 = bf16[512,512]{1,0:T(8,128)(2,1)} copy(bf16[512,512]{1,0:T(8,128)(2,1)S(1)} %mixer.1) | data formatting | bytes 1048576

commit v7 on v6

--- a/solution.py
+++ b/solution.py
@@ -540,16 +540,15 @@
             combine(pieces[i][0], pieces[i][1], False)
 
     def pack(one, two):
-        one = jnp.sum(one, axis=1, keepdims=True)
-        two = jnp.sum(two, axis=1, keepdims=True)
-        lane = lax.broadcasted_iota(jnp.int32, (rows, 128), 1)
-        return jnp.transpose(jnp.where(lane == 0, one, jnp.where(lane == 1, two, 0.0)))[0:8]
+        one = jnp.sum(jnp.transpose(one), axis=0, keepdims=True)
+        two = jnp.sum(jnp.transpose(two), axis=0, keepdims=True)
+        return jnp.concatenate([one, two, jnp.zeros((6, rows), f32)], axis=0)
 
     sums[...] = jnp.zeros_like(sums)
     emits = {5: (6, 8), 7: (8, 10), 9: (10, 12), 11: (12, 14), 12: (14, 15), 13: (15, 16)}
     odd = lax.rem(t, 2) == 1
     ahead = {6: (6, 8), 7: (8, 10), 9: (10, 12), 11: (12, 14), 12: (14, 15), 13: (15, 16)}
-    behind = {7: (6, 8), 8: (8, 10), 10: (10, 12), 13: (12, 16)}
+    behind = {7: (6, 8), 8: (8, 10), 10: (10, 12), 12: (12, 14), 13: (14, 16)}
 
     def on(core, work, *args):
         @pl.when(odd == core)
@@ -662,12 +661,12 @@
     totals = late[...] + stats[0]
     for i in range(1, tp):
         totals = totals + stats[i]
-    tall = jnp.concatenate([totals, jnp.zeros((120, rows), f32)], axis=0)
+    width = gain_ref.shape[1] * tp
+    line_mean = totals[0:1] / width
+    line_scale = lax.rsqrt(totals[1:2] / width - line_mean * line_mean + epsilon)
+    tall = jnp.concatenate([line_mean, line_scale, jnp.zeros((126, rows), f32)], axis=0)
     back = jnp.transpose(tall)
-    width = gain_ref.shape[1] * tp
-    row_mean = back[:, 0:1] / width
-    variance = back[:, 1:2] / width - row_mean * row_mean
-    scale = lax.rsqrt(variance + epsilon)
+    row_mean, scale = back[:, 0:1], back[:, 1:2]
     normed = ((acc[:, 0 : gain_ref.shape[1]] - row_mean) * scale * gains[...]).astype(bf16)
     for b in range(blocks):
         out_ref[b * WINDOW : (b + 1) * WINDOW, :] = normed[place(b) : place(b) + WINDOW]

time: 60.5 us -> 60.4 us (level)
  no operation moved by 1% of the time
where the time goes in v7:
time: 60.4 us; the launch traced here: 59.9 us
  Pallas kernels  59.1 us (98%)
  local copies, waits for them, and re-layouts  0.8 us (1%)
    pallas_call x1, Pallas kernels, fused(): pl.pallas_call(functools.partial(mixer_kernel, n, tp), out_shape=jax.Shap...  59.1 us

profile of v7, /device:TPU:0, one launch (start us, length us, event | category | flops | bytes accessed | tf_op | source)
XLA Modules:
  0.0 59.9 jit_solution(1660974815523126973)
XLA Ops:
  0.0 59.1 %mixer.1 = bf16[512,512]{1,0:T(8,128)(2,1)S(1)} custom-call(bf16[512,512]{1,0:T(8,128)(2,1)} %tok_ref.1, bf16[4,64,256]{2,1,0:T(8,128)(2,1)} %bitcast.7, bf16[64,256]{1,0:T(8,128)(2,1)} %bitcast.9, bf16[64,256]{1,0:T(8,128)(2,1)} %bitcast.10, bf16[4,64,256]{2,1,0:T(8,128)(2,1)} %bitcast.8, f32[1,4]{1,0:T(1,128)} %bitcast.13, bf16[1,256,256]{2,1,0:T(8,128)(2,1)} %wp_ref.1, ...), custom_call_target="tpu_custom_call" | custom-call | tf_op jit(solution)/shard_map/mixer/pallas_call | solution.py:690
  59.1 0.8 %copy.13 = bf16[512,512]{1,0:T(8,128)(2,1)} copy(bf16[512,512]{1,0:T(8,128)(2,1)S(1)} %mixer.1) | data formatting | bytes 1048576

commit v8 on v7

--- a/solution.py
+++ b/solution.py
@@ -249,22 +249,30 @@
 
     loads = []
 
-    def fetch(src, dst):
-        copy = pltpu.make_async_copy(src, dst, load.at[len(loads)])
+    def fetch(src, dst, sem=None):
+        copy = pltpu.make_async_copy(src, dst, load.at[len(loads)] if sem is None else load.at[sem])
         copy.start()
-        loads.append(copy)
+        if sem is None:
+            loads.append(copy)
         return copy
 
-    pairs = [fetch(wk_ref, pair_in.at[pl.ds(0, kc)]), fetch(wv_ref, pair_in.at[pl.ds(kc, kc)])]
+    fetch(wk_ref, pair_in.at[pl.ds(0, kc)])
+    fetch(wv_ref, pair_in.at[pl.ds(kc, kc)], 0)
+    pairs = [pltpu.make_async_copy(pair_in, pair_in, load.at[0])]
     first = [
         fetch(wq_ref, win.at[me, :, :, pl.ds(0, qc)]),
         fetch(wc_ref, win.at[me, :, :, pl.ds(qc + 2 * kc, cc)]),
     ]
-    own_tok = [fetch(tok_ref.at[:, pl.ds(b * depth, depth)], tok.at[t * per + b]) for b in range(per)]
-    later = []
+    mine = tok.at[pl.ds(t * per, per)]
+    own_sem = len(loads)
+    for b in range(per):
+        fetch(tok_ref.at[:, pl.ds(b * depth, depth)], tok.at[t * per + b], own_sem if b else None)
+    own_tok = [pltpu.make_async_copy(mine, mine, load.at[own_sem])]
+    wout_sem = len(loads)
     for h in range(2):
-        later.append(fetch(woa_ref.at[:, pl.ds(h * half, half)], wout.at[me, h, 0]))
-        later.append(fetch(wop_ref.at[:, pl.ds(h * half, half)], wout.at[me, h, 1]))
+        fetch(woa_ref.at[:, pl.ds(h * half, half)], wout.at[me, h, 0], wout_sem if h else None)
+        fetch(wop_ref.at[:, pl.ds(h * half, half)], wout.at[me, h, 1], wout_sem)
+    later = [pltpu.make_async_copy(wout.at[me], wout.at[me], load.at[wout_sem])]
     later.append(fetch(sink_ref, sinks))
     later.append(fetch(wp_ref, wpool))
     later.append(fetch(ps_ref, scales))
@@ -485,6 +493,13 @@
 
     def to_late():
         return rdma(late, late, late_send.at[0], late_recv.at[0], me, mate)
+
+    def to_far():
+        return rdma(late, late, late_send.at[1], late_recv.at[0], me, lax.rem(mate + 2, tp))
+
+    detour = holder == 0
+    tells = jnp.logical_or(holder == across, jnp.logical_and(holder == t, jnp.logical_not(detour)))
+    tells_far = jnp.logical_and(holder == across, detour)
 
     pieces = [(0, 0), (0, 1)]
     for k in range(1, count - 2, 2):
@@ -622,7 +637,10 @@
             acc[:, pl.ds(pl.multiple_of((2 * i + h) * half, 128), half)] = mix
             one, two = one + mix, two + mix * mix
         late[...] = pack(one, two)
-        to_late().start()
+
+        @pl.when(tells)
+        def _():
+            to_late().start()
 
     @pl.when(holder == across)
     def _():
@@ -632,23 +650,17 @@
             mix = part[final, h].astype(f32) + echo[h].astype(f32)
             one, two = one + mix, two + mix * mix
         late[...] = pack(one, two)
+
+        @pl.when(tells_far)
+        def _():
+            to_far().start()
+
         to_late().start()
 
     def drain(buf, amount, sem):
         whole = buf.at[pl.ds(0, amount)]
         rdma(whole, whole, sem.at[0], mate_recv.at[0, 0], me, mate).wait_send()
 
-    drain(part, n // 2, mate_send)
-    drain(part, per, part_send)
-    drain(tok, 3 * per, tok_send)
-
-    @pl.when(holder == t)
-    def _():
-        drain(part, 1, echo_send)
-
-    for turn in range(2 * count - SENDS, 2 * count):
-        for way in range(2):
-            launched(way, turn).wait_send()
     for j in range(1, tp):
         src = lax.rem(t + j, tp)
         rdma(stats.at[src], stats.at[src], stat_send.at[0], stat_recv.at[src], me, src).wait_recv()
@@ -664,17 +676,32 @@
     width = gain_ref.shape[1] * tp
     line_mean = totals[0:1] / width
     line_scale = lax.rsqrt(totals[1:2] / width - line_mean * line_mean + epsilon)
-    tall = jnp.concatenate([line_mean, line_scale, jnp.zeros((126, rows), f32)], axis=0)
+    tall = jnp.concatenate([line_mean, line_scale, jnp.zeros((6, rows), f32)], axis=0)
     back = jnp.transpose(tall)
     row_mean, scale = back[:, 0:1], back[:, 1:2]
     normed = ((acc[:, 0 : gain_ref.shape[1]] - row_mean) * scale * gains[...]).astype(bf16)
     for b in range(blocks):
         out_ref[b * WINDOW : (b + 1) * WINDOW, :] = normed[place(b) : place(b) + WINDOW]
+    drain(part, n // 2, mate_send)
+    drain(part, per, part_send)
+    drain(tok, 3 * per, tok_send)
+
+    @pl.when(holder == t)
+    def _():
+        drain(part, 1, echo_send)
+
+    for turn in range(2 * count - SENDS, 2 * count):
+        for way in range(2):
+            launched(way, turn).wait_send()
     drain(stats, tp - 1, stat_send)
 
-    @pl.when(paired)
+    @pl.when(tells)
     def _():
         to_late().wait_send()
+
+    @pl.when(tells_far)
+    def _():
+        to_far().wait_send()
 
 
 def fused(n, tp, tokens, w_query, w_key, w_value, w_pool_in, sink, w_pool, pool_scale, w_out_attn, w_out_pool, out_gain):
@@ -726,10 +753,10 @@
             dma((per, 2)),
             dma((1,)),
             dma((2,)),
-            dma((per + 12,)),
+            dma((9,)),
             dma((1,)),
             dma((tp,)),
-            dma((1,)),
+            dma((2,)),
             dma((1,)),
         ],
         compiler_params=pltpu.CompilerParams(

time: 60.4 us -> 60 us (level)
  no operation moved by 1% of the time
where the time goes in v8:
time: 60 us; the launch traced here: 59.9 us
  Pallas kernels  59.1 us (98%)
  local copies, waits for them, and re-layouts  0.8 us (1%)
    pallas_call x1, Pallas kernels, fused(): pl.pallas_call(functools.partial(mixer_kernel, n, tp), out_shape=jax.Shap...  59.1 us

profile of v8, /device:TPU:0, one launch (start us, length us, event | category | flops | bytes accessed | tf_op | source)
XLA Modules:
  0.0 59.9 jit_solution(4568628405422497115)
XLA Ops:
  0.0 59.1 %mixer.1 = bf16[512,512]{1,0:T(8,128)(2,1)S(1)} custom-call(bf16[512,512]{1,0:T(8,128)(2,1)} %tok_ref.1, bf16[4,64,256]{2,1,0:T(8,128)(2,1)} %bitcast.7, bf16[64,256]{1,0:T(8,128)(2,1)} %bitcast.9, bf16[64,256]{1,0:T(8,128)(2,1)} %bitcast.10, bf16[4,64,256]{2,1,0:T(8,128)(2,1)} %bitcast.8, f32[1,4]{1,0:T(1,128)} %bitcast.13, bf16[1,256,256]{2,1,0:T(8,128)(2,1)} %wp_ref.1, ...), custom_call_target="tpu_custom_call" | custom-call | tf_op jit(solution)/shard_map/mixer/pallas_call | solution.py:717
  59.1 0.8 %copy.13 = bf16[512,512]{1,0:T(8,128)(2,1)} copy(bf16[512,512]{1,0:T(8,128)(2,1)S(1)} %mixer.1) | data formatting | bytes 1048576

commit v9 on v8

--- a/solution.py
+++ b/solution.py
@@ -563,7 +563,8 @@
     emits = {5: (6, 8), 7: (8, 10), 9: (10, 12), 11: (12, 14), 12: (14, 15), 13: (15, 16)}
     odd = lax.rem(t, 2) == 1
     ahead = {6: (6, 8), 7: (8, 10), 9: (10, 12), 11: (12, 14), 12: (14, 15), 13: (15, 16)}
-    behind = {7: (6, 8), 8: (8, 10), 10: (10, 12), 12: (12, 14), 13: (14, 16)}
+    behind = {7: (6, 8), 8: (8, 10), 10: (10, 12), 13: (14, 16)}
+    soon = lax.rem(holder, 2) == 1
 
     def on(core, work, *args):
         @pl.when(odd == core)
@@ -596,6 +597,12 @@
             on(True, combine_near, 1)
         if k in ahead:
             on(False, combine_far, range(*ahead[k]))
+        if k >= last - 1:
+
+            @pl.when(jnp.logical_and(odd, soon == (k == last - 1)))
+            def _():
+                combine_far(range(12, 14))
+
         if k in behind:
             on(True, combine_far, range(*behind[k]))
 

time: 60 us -> 60 us (level)
  no operation moved by 1% of the time
where the time goes in v9:
time: 60 us; the launch traced here: 59.9 us
  Pallas kernels  59.1 us (98%)
  local copies, waits for them, and re-layouts  0.8 us (1%)
    pallas_call x1, Pallas kernels, fused(): pl.pallas_call(functools.partial(mixer_kernel, n, tp), out_shape=jax.Shap...  59.1 us

profile of v9, /device:TPU:0, one launch (start us, length us, event | category | flops | bytes accessed | tf_op | source)
XLA Modules:
  0.0 59.9 jit_solution(5343482675056737487)
XLA Ops:
  0.0 59.1 %mixer.1 = bf16[512,512]{1,0:T(8,128)(2,1)S(1)} custom-call(bf16[512,512]{1,0:T(8,128)(2,1)} %tok_ref.1, bf16[4,64,256]{2,1,0:T(8,128)(2,1)} %bitcast.7, bf16[64,256]{1,0:T(8,128)(2,1)} %bitcast.9, bf16[64,256]{1,0:T(8,128)(2,1)} %bitcast.10, bf16[4,64,256]{2,1,0:T(8,128)(2,1)} %bitcast.8, f32[1,4]{1,0:T(1,128)} %bitcast.13, bf16[1,256,256]{2,1,0:T(8,128)(2,1)} %wp_ref.1, ...), custom_call_target="tpu_custom_call" | custom-call | tf_op jit(solution)/shard_map/mixer/pallas_call | solution.py:724
  59.1 0.8 %copy.13 = bf16[512,512]{1,0:T(8,128)(2,1)} copy(bf16[512,512]{1,0:T(8,128)(2,1)S(1)} %mixer.1) | data formatting | bytes 1048576
